TPU v7x, 128 devices: a whole 4x4x4 slice. The times are simulated.
128 devices in a mesh: ep: 64 (over z, y, x), tp: 2 (over core).
Axes of the slice: x: 4, y: 4, z: 4, core: 2. Of those that a mesh axis runs over, the one named last changes fastest.
Arguments:
- tokens: bfloat16 [1024, 2048], P('ep'), may hold values from -6 to 6
- norm_gain: bfloat16 [2048], replicated, may hold values from 0.099609375 to 1.8984375
- w_query: bfloat16 [2048, 512], P(None, 'tp'), may hold values from -0.125 to 0.125
- w_key: bfloat16 [2048, 256], P(None, 'tp'), may hold values from -0.125 to 0.125
- w_value: bfloat16 [2048, 256], P(None, 'tp'), may hold values from -0.125 to 0.125
- w_forget: bfloat16 [2048, 8], P(None, 'tp'), may hold values from -0.25 to 0.25
- w_out: bfloat16 [512, 2048], P('tp'), may hold values from -0.25 to 0.25
- cache_keys: bfloat16 [1024, 1024, 256], P('ep', None, 'tp'), may hold values from -700 to 700
- cache_values: bfloat16 [1024, 1024, 256], P('ep', None, 'tp'), may hold values from -6 to 6
- cache_gates: float32 [1024, 8, 1024], P('ep', 'tp'), as said below
- lengths: int32 [1024], P('ep'), may hold values from 1 to 1024, as said below
- ffn_gain: bfloat16 [2048], replicated, may hold values from 0.099609375 to 1.8984375
- router_w: bfloat16 [2048, 64], replicated, may hold values from -0.125 to 0.125
- routes: int32 [1024, 6], P('ep'), may hold values from 0 to 63, all different within a row; in each aligned block of 16 rows (0 to 15, 16 to 31, ...) at most 3 rows name the same one
- shared_gate: bfloat16 [2048, 512], P(None, 'tp'), may hold values from -0.125 to 0.125
- shared_up: bfloat16 [2048, 512], P(None, 'tp'), may hold values from -0.125 to 0.125
- shared_down: bfloat16 [512, 2048], P('tp'), may hold values from -0.25 to 0.25
- expert_gate: bfloat16 [64, 2048, 512], P('ep', None, 'tp'), may hold values from -0.125 to 0.125
- expert_up: bfloat16 [64, 2048, 512], P('ep', None, 'tp'), may hold values from -0.125 to 0.125
- expert_down: bfloat16 [64, 512, 2048], P('ep', 'tp'), may hold values from -0.25 to 0.25
Outputs:
- layer_out: bfloat16 [1024, 2048], P('ep')
Inputs may be any that keep to these rules, and one draw needn't show every extreme that they name: `routes`: each row names 6 different experts. Among the rows of one index of ep no expert is named by more than 3 rows, and in every draw some expert is named by exactly 3 of them. `lengths`: in every draw some sequence has all 1024 positions. `cache_gates`: each row is non-increasing along the positions.
All inputs are finite; a program needn't handle non-finite values.
Results may differ from a plain program's by a relative error of at most 0.017.
Values may be sent and summed in bfloat16 or wider, within the bound.
A program may use at most 64 MiB of HBM per device.

v0:
```python
import jax
import jax.numpy as jnp
from jax import lax
from jax.sharding import PartitionSpec as P

HEAD_DIM = 64


EPS = 1e-06
ROUTE_SCALE = 2.5


def total_of_pieces(array, axis):
    parts = lax.all_gather(array, axis).astype(jnp.float32)
    return parts.sum(axis=0)


def copy_for_each(array, axis):
    size = lax.axis_size(axis)
    return lax.all_to_all(
        jnp.broadcast_to(array[None], (size, *array.shape)), axis, 0, 0, tiled=True
    )


def over_copies(array, axis):
    everything = copy_for_each(array, axis)
    return jnp.sum(everything.astype(jnp.float32), axis=0)


def norm_rows(rows, norm_gain):
    values = rows.astype(jnp.float32)
    factor = lax.rsqrt(jnp.mean(values * values, axis=-1, keepdims=True) + EPS)
    return (values * factor * norm_gain.astype(jnp.float32)).astype(jnp.bfloat16)


def swiglu_hidden(rows, w_gate, w_up):
    gate_proj = jnp.dot(rows, w_gate, preferred_element_type=jnp.float32)
    upward = jnp.dot(rows, w_up, preferred_element_type=jnp.float32)
    return (jax.nn.silu(gate_proj) * upward).astype(jnp.bfloat16)


def route_weights(rows, router_w, chosen):
    scores = jax.nn.sigmoid(jnp.dot(rows, router_w, preferred_element_type=jnp.float32))
    picked = jnp.take_along_axis(scores, chosen, axis=1)
    return ROUTE_SCALE * picked / jnp.sum(picked, axis=1, keepdims=True)


def slot_hidden(incoming, expert_gate, expert_up):
    gate_proj = jnp.einsum(
        "scd,df->scf", incoming, expert_gate[0], preferred_element_type=jnp.float32
    )
    upward = jnp.einsum("scd,df->scf", incoming, expert_up[0], preferred_element_type=jnp.float32)
    return (jax.nn.silu(gate_proj) * upward).astype(jnp.bfloat16)


def attend(
    normed, w_query, w_key, w_value, w_forget, cache_keys, cache_values, cache_gates, lengths
):
    seq_count = normed.shape[0]
    head_count = w_forget.shape[1]
    kv_count = w_key.shape[1] // HEAD_DIM
    group_size = head_count // kv_count
    cache_len = cache_keys.shape[1]
    score_scale = HEAD_DIM ** (-0.5)
    queries = jnp.dot(normed, w_query, preferred_element_type=jnp.float32).astype(jnp.bfloat16)
    queries = queries.reshape(seq_count, kv_count, group_size, HEAD_DIM)
    key_new = jnp.dot(normed, w_key, preferred_element_type=jnp.float32).astype(jnp.bfloat16)
    key_new = key_new.reshape(seq_count, kv_count, HEAD_DIM)
    value_new = jnp.dot(normed, w_value, preferred_element_type=jnp.float32).astype(jnp.bfloat16)
    value_new = value_new.reshape(seq_count, kv_count, HEAD_DIM)
    log_gate = jax.nn.log_sigmoid(jnp.dot(normed, w_forget, preferred_element_type=jnp.float32))
    cached_keys = cache_keys.reshape(seq_count, cache_len, kv_count, HEAD_DIM)
    cached_values = cache_values.reshape(seq_count, cache_len, kv_count, HEAD_DIM)
    past_score = (
        jnp.einsum("skgd,slkd->skgl", queries, cached_keys, preferred_element_type=jnp.float32)
        * score_scale
    )
    last_index = jnp.broadcast_to((lengths - 1)[:, None, None], (seq_count, head_count, 1))
    last_gate = jnp.take_along_axis(cache_gates, last_index, axis=2)
    gate_bias = last_gate + log_gate[:, :, None] - cache_gates
    past_score = past_score + gate_bias.reshape(seq_count, kv_count, group_size, cache_len)
    is_valid = jnp.arange(cache_len)[None, :] < lengths[:, None]
    past_score = jnp.where(is_valid[:, None, None, :], past_score, -jnp.inf)
    self_score = (
        jnp.einsum("skgd,skd->skg", queries, key_new, preferred_element_type=jnp.float32)
        * score_scale
    )
    peak_score = jnp.maximum(jnp.max(past_score, axis=-1), self_score)
    past_weight = jnp.exp(past_score - peak_score[..., None])
    self_weight = jnp.exp(self_score - peak_score)
    weight_sum = jnp.sum(past_weight, axis=-1) + self_weight
    past_prob = (past_weight / weight_sum[..., None]).astype(jnp.bfloat16)
    self_prob = (self_weight / weight_sum).astype(jnp.bfloat16)
    mixed_heads = jnp.einsum(
        "skgl,slkd->skgd", past_prob, cached_values, preferred_element_type=jnp.float32
    )
    mixed_heads = (
        mixed_heads
        + self_prob.astype(jnp.float32)[..., None] * value_new.astype(jnp.float32)[:, :, None, :]
    )
    return mixed_heads.astype(jnp.bfloat16).reshape(seq_count, head_count * HEAD_DIM)


def per_device(
    tokens,
    norm_gain,
    w_query,
    w_key,
    w_value,
    w_forget,
    w_out,
    cache_keys,
    cache_values,
    cache_gates,
    lengths,
    ffn_gain,
    router_w,
    routes,
    shared_gate,
    shared_up,
    shared_down,
    expert_gate,
    expert_up,
    expert_down,
):
    seq_count = tokens.shape[0]
    width = tokens.shape[1]
    top_k = routes.shape[1]
    groups = lax.axis_size("ep")
    capacity = max(2, 2 * seq_count * top_k // groups)
    normed = norm_rows(tokens, norm_gain)
    attn = attend(
        normed, w_query, w_key, w_value, w_forget, cache_keys, cache_values, cache_gates, lengths
    )
    partial_value = jnp.dot(attn, w_out, preferred_element_type=jnp.float32)
    attended = total_of_pieces(partial_value.astype(jnp.bfloat16), "tp").astype(jnp.float32)
    residual_rows = (tokens.astype(jnp.float32) + attended).astype(jnp.bfloat16)
    ffn_rows = norm_rows(residual_rows, ffn_gain)
    shared_part = jnp.dot(
        swiglu_hidden(ffn_rows, shared_gate, shared_up),
        shared_down,
        preferred_element_type=jnp.float32,
    )
    flat_routes = routes.reshape(-1)
    expert_marks = (flat_routes[:, None] == jnp.arange(groups, dtype=jnp.int32)[None, :]).astype(
        jnp.int32
    )
    before = jnp.cumsum(expert_marks, axis=0) - expert_marks
    slot_rank = jnp.sum(before * expert_marks, axis=1)
    target = flat_routes * capacity + slot_rank
    sources = jnp.repeat(ffn_rows, top_k, axis=0)
    outgoing = jnp.zeros((groups * capacity, width), jnp.bfloat16).at[target].set(sources)
    outgoing = outgoing.reshape(groups, capacity, width)
    weights = route_weights(ffn_rows, router_w, routes)
    shared = over_copies(shared_part.astype(jnp.bfloat16), "tp").astype(jnp.float32)
    hidden = slot_hidden(
        lax.all_to_all(outgoing, "ep", split_axis=0, concat_axis=0, tiled=True),
        expert_gate,
        expert_up,
    )
    part_rows = jnp.einsum(
        "scf,fd->scd", hidden, expert_down[0], preferred_element_type=jnp.float32
    )
    merged = (
        over_copies(part_rows.astype(jnp.bfloat16), "tp").astype(jnp.float32).astype(jnp.bfloat16)
    )
    returned = lax.all_to_all(merged, "ep", split_axis=0, concat_axis=0, tiled=True)
    answers = returned.reshape(groups * capacity, width)[target].astype(jnp.float32)
    routed = jnp.sum((answers * weights.reshape(-1, 1)).reshape(seq_count, top_k, width), axis=1)
    return (residual_rows.astype(jnp.float32) + shared + routed).astype(jnp.bfloat16)


def solution(mesh):
    placed = (
        P("ep", None),
        P(),
        P(None, "tp"),
        P(None, "tp"),
        P(None, "tp"),
        P(None, "tp"),
        P("tp", None),
        P("ep", None, "tp"),
        P("ep", None, "tp"),
        P("ep", "tp", None),
        P("ep"),
        P(),
        P(),
        P("ep", None),
        P(None, "tp"),
        P(None, "tp"),
        P("tp", None),
        P("ep", None, "tp"),
        P("ep", None, "tp"),
        P("ep", "tp", None),
    )
    return jax.shard_map(
        per_device, mesh=mesh, in_specs=placed, out_specs=P("ep", None), check_vma=False
    )
```

profile of v0, /device:TPU:1, one launch (start us, length us, event | category | flops | bytes accessed | tf_op | source)
XLA Modules:
  0.0 109.4 jit_solution(15329260007453169757)
XLA Ops:
  0.0 0.7 broadcast_add_fusion
  0.7 0.7 broadcast_compare_fusion
  1.4 0.7 iota_compare_fusion
  2.1 0.8 copy.86
  2.9 0.7 broadcast_multiply_fusion
  3.6 0.1 copy.81
  3.7 0.1 reshape.276
  3.9 2.0 %gather_fusion.1 = f32[64]{0:T(128)S(1)} fusion(f32[16,4,1024]{2,1,0:T(4,128)} %param.29, s32[64]{0:T(128)S(1)} %reshape.276), kind=kCustom, calls=%fused_computation.1 | custom fusion | bytes 1280 | tf_op jit(solution)/shard_map/jit(take_along_axis)/gather | solution.py:79
  6.0 0.1 copy.82
  6.1 0.1 fusion.25
  6.3 0.2 fusion.46
  6.5 0.1 copy.83
  6.6 0.1 broadcast_subtract_fusion
  6.7 0.2 reshape.256
  6.9 0.3 convolution_convert_fusion.3
  7.2 0.1 reshape.254
  7.3 6.5 %copy.80 = bf16[16,1024,128]{1,2,0:T(8,128)(2,1)} copy(bf16[16,1024,128]{2,1,0:T(8,128)(2,1)} %param.27) | data formatting | bytes 8388608 | tf_op args[7]
  13.8 0.2 convolution_convert_fusion.5
  14.0 0.1 reshape.311
  14.1 0.2 fusion.64
  14.3 3.0 %fusion.63 = (f32[16,2,2]{2,1,0:T(2,128)S(1)}, f32[16,2,2,1024]{3,2,1,0:T(2,128)S(1)}) fusion(f32[16,2,2,1024]{3,2,1,0:T(2,128)S(1)} %reshape.256, bf16[16,2,2,64]{3,2,1,0:T(2,128)(2,1)S(1)} %reshape.254, bf16[16,1024,2,64]{1,3,2,0:T(8,128)(2,1)} %bitcast.51, pred[16,1024]{1,0:T(8,128)(4,1)S(1)} %iota_compare_fusion), kind=kOutput, calls=%fused_computation.111 | convolution fusion | flops 8650688 | bytes 4743424 | tf_op jit(solution)/shard_map/skgd,slkd->skgl/dot_general | solution.py:75
  17.3 0.3 fusion.24
  17.7 0.2 fusion.8
  18.0 6.4 %copy.84 = bf16[16,1024,128]{1,2,0:T(8,128)(2,1)} copy(bf16[16,1024,128]{2,1,0:T(8,128)(2,1)} %param.28) | data formatting | bytes 8388608 | tf_op args[8]
  24.4 3.5 %fusion.3 = bf16[16,2,2,64]{3,2,1,0:T(2,128)(2,1)S(1)} fusion(bf16[16,1024,2,64]{1,3,2,0:T(8,128)(2,1)} %bitcast.52, f32[16,2,2,1024]{3,2,1,0:T(2,128)S(1)} %get-tuple-element.12, f32[16,2,2]{2,1,0:T(2,128)S(1)} %get-tuple-element.8, f32[16,2,2]{2,1,0:T(2,128)S(1)} %multiply_maximum_fusion, f32[16,2,64]{2,1,0:T(2,128)S(1)} %reshape.264, ...), kind=kOutput, calls=%fused_computation.13 | convolution fusion | flops 8597504 | bytes 4473600 | tf_op jit(solution)/shard_map/skgl,slkd->skgd/dot_general | solution.py:94
  27.9 0.1 reshape.259
  28.0 0.2 convolution_convert_fusion.2
  28.3 3.1 %all-gather = bf16[32,2048]{1,0:T(8,128)(2,1)S(1)} all-gather(bf16[16,2048]{1,0:T(8,128)(2,1)S(1)} %convolution_convert_fusion.2), channel_id=2, replica_groups=mesh['ep'=64,'tp'=2] {'tp'}, dimensions={0}, use_global_device_ids=true | all-gather | bytes 196608 | tf_op jit(solution)/shard_map/all_gather | solution.py:14
  31.4 0.1 fusion.29
  31.5 0.1 fusion.31
  31.7 0.1 reshape.292
  31.8 0.1 eq.15
  31.9 0.1 fusion.37
  32.0 0.1 reduce_window_sum.11
  32.1 0.2 select_reduce_fusion
  32.3 0.1 copy.85
  32.4 0.1 mul.136
  32.5 1.4 %scatter_custom_fusion = bf16[192,2048]{1,0:T(8,128)(2,1)S(1)} fusion(s32[96]{0:T(128)S(1)} %fusion.53, bf16[96,2048]{1,0:T(8,128)(2,1)S(1)} %reshape.292, bf16[]{:T(256)} %constant.64.clone.1), kind=kCustom, calls=%fused_computation.32 | custom fusion | bytes 786434 | tf_op jit(solution)/shard_map/scatter | solution.py:152
  34.0 1.3 %reshape.261 = bf16[64,3,2048]{2,1,0:T(4,128)(2,1)} reshape(bf16[192,2048]{1,0:T(8,128)(2,1)S(1)} %scatter_custom_fusion) | data formatting | bytes 1572864 | tf_op jit(solution)/shard_map/reshape | solution.py:153
  35.3 11.5 %all-to-all-start.1 = ((bf16[64,3,2048]{2,1,0:T(4,128)(2,1)}), bf16[64,3,2048]{2,1,0:T(4,128)(2,1)}, u32[]{:S(2)}, u32[]{:S(2)}) async-start(bf16[64,3,2048]{2,1,0:T(4,128)(2,1)} %reshape.261), calls=%async_computation.1 | async-start | bytes 2097152 | tf_op jit(solution)/shard_map/all_to_all | solution.py:157
  46.8 0.1 copy.90
  46.9 0.1 reshape.282
  47.0 0.2 fusion.65
  47.2 2.3 %convolution_convert_fusion.1 = bf16[16,2048]{1,0:T(8,128)(2,1)S(1)} fusion(bf16[256,2048]{1,0:T(8,128)(2,1)} %param.36, bf16[16,2048]{1,0:T(8,128)(2,1)S(1)} %fusion.31, bf16[2048,256]{1,0:T(8,128)(2,1)} %param.35, f32[16,256]{1,0:T(8,128)S(1)} %fusion.65), kind=kOutput, calls=%fused_computation.5 | convolution fusion | flops 33611776 | bytes 2244608 | tf_op jit(solution)/shard_map/dot_general | solution.py:139
  49.5 15.2 %all-to-all-done.1 = bf16[64,3,2048]{2,1,0:T(4,128)(2,1)} async-done(((bf16[64,3,2048]{2,1,0:T(4,128)(2,1)}), bf16[64,3,2048]{2,1,0:T(4,128)(2,1)}, u32[]{:S(2)}, u32[]{:S(2)}) %all-to-all-start.1) | async-done | bytes 786464 | tf_op jit(solution)/shard_map/all_to_all | solution.py:157
  64.7 2.5 %fusion.12 = f32[64,3,256]{2,0,1:T(8,128)S(1)} fusion(bf16[1,2048,256]{2,1,0:T(8,128)(2,1)} %param.37, bf16[64,3,2048]{2,1,0:T(4,128)(2,1)} %all-to-all-done.1), kind=kOutput, calls=%fused_computation.27 | convolution fusion | flops 201326592 | bytes 2031616 | tf_op jit(solution)/shard_map/scd,df->scf/dot_general | solution.py:49
  67.2 2.7 %convolution_convert_fusion = bf16[64,3,2048]{2,0,1:T(8,128)(2,1)S(1)} fusion(bf16[1,256,2048]{2,1,0:T(8,128)(2,1)S(1)} %copy-done, bf16[1,2048,256]{2,1,0:T(8,128)(2,1)} %param.38, bf16[64,3,2048]{2,1,0:T(4,128)(2,1)} %all-to-all-done.1, f32[64,3,256]{2,0,1:T(8,128)S(1)} %fusion.12), kind=kOutput, calls=%fused_computation.4 | convolution fusion | flops 403341312 | bytes 3866624 | tf_op jit(solution)/shard_map/scf,fd->scd/dot_general | solution.py:161
  70.0 0.2 broadcast_in_dim.82
  70.2 6.4 %all_to_all.20 = bf16[2,64,3,2048]{3,1,2,0:T(8,128)(2,1)S(1)} all-to-all(bf16[2,64,3,2048]{3,1,2,0:T(8,128)(2,1)S(1)} %broadcast_in_dim.82), channel_id=1, replica_groups=mesh['ep'=64,'tp'=2] {'tp'}, dimensions={0} | all-to-all | bytes 3145728 | tf_op jit(solution)/shard_map/all_to_all | solution.py:20
  76.6 0.7 broadcast_in_dim.79
  77.2 4.4 %all-to-all-start = ((bf16[2,16,2048]{2,1,0:T(8,128)(2,1)}), bf16[2,16,2048]{2,1,0:T(8,128)(2,1)}, u32[]{:S(2)}, u32[]{:S(2)}) async-start(bf16[2,16,2048]{2,1,0:T(8,128)(2,1)} %broadcast_in_dim.79), calls=%async_computation | async-start | bytes 262144 | tf_op jit(solution)/shard_map/all_to_all | solution.py:20
  81.6 0.4 reduce_sum.93
  82.0 1.7 %copy.89 = bf16[64,3,2048]{2,1,0:T(4,128)(2,1)} copy(bf16[64,3,2048]{2,0,1:T(8,128)(2,1)S(1)} %reduce_sum.93) | data formatting | bytes 1572864 | tf_op jit(solution)/shard_map/reduce_sum | solution.py:27
  83.6 4.7 %all-to-all-start.3 = ((bf16[64,3,2048]{2,1,0:T(4,128)(2,1)}), bf16[64,3,2048]{2,1,0:T(4,128)(2,1)S(1)}, u32[]{:S(2)}, u32[]{:S(2)}) async-start(bf16[64,3,2048]{2,1,0:T(4,128)(2,1)} %copy.89), calls=%async_computation.3 | async-start | bytes 2097152 | tf_op jit(solution)/shard_map/all_to_all | solution.py:167
  88.3 1.1 %fusion.7 = f32[16,64]{1,0:T(8,128)S(1)} fusion(bf16[16,2048]{1,0:T(8,128)(2,1)S(1)} %fusion.31, bf16[2048,64]{0,1:T(8,128)(2,1)} %param.32), kind=kOutput, calls=%fused_computation.20 | convolution fusion | flops 4197376 | bytes 331776 | tf_op jit(solution)/shard_map/dot_general | solution.py:43
  89.4 1.3 %gather_fusion.2 = f32[96]{0:T(128)S(1)} fusion(f32[16,64]{1,0:T(8,128)S(1)} %fusion.7, s32[96]{0:T(128)S(1)} %reshape.282), kind=kCustom, calls=%fused_computation.2 | custom fusion | bytes 1536 | tf_op jit(solution)/shard_map/jit(take_along_axis)/gather | solution.py:44
  90.9 0.1 copy.92
  91.0 0.9 convert_reduce_fusion.1
  92.0 14.7 %all-to-all-done.3 = bf16[64,3,2048]{2,1,0:T(4,128)(2,1)S(1)} async-done(((bf16[64,3,2048]{2,1,0:T(4,128)(2,1)}), bf16[64,3,2048]{2,1,0:T(4,128)(2,1)S(1)}, u32[]{:S(2)}, u32[]{:S(2)}) %all-to-all-start.3) | async-done | bytes 786464 | tf_op jit(solution)/shard_map/all_to_all | solution.py:167
  106.7 0.7 reshape.262
  107.4 0.8 gather_fusion
  108.2 0.1 reshape.265
  108.3 0.4 multiply_reduce_fusion
  108.7 0.7 fusion.33
  (47 shorter events, 0.6 us)
Async XLA Ops:
  0.0 67.2 %copy-start = (bf16[1,256,2048]{2,1,0:T(8,128)(2,1)S(1)}, bf16[1,256,2048]{2,1,0:T(8,128)(2,1)}, u32[]{:S(2)}) copy-start(bf16[1,256,2048]{2,1,0:T(8,128)(2,1)} %param.39) | copy-start | bytes 3145732
  3.8 2.3 %copy-start.9 = (bf16[2048]{0:T(1024)(128)(2,1)S(1)}, bf16[2048]{0:T(1024)(128)(2,1)}, u32[]{:S(2)}) copy-start(bf16[2048]{0:T(1024)(128)(2,1)} %param.21) | copy-start | bytes 12292
  3.8 2.3 %copy-start.2 = (bf16[16,2048]{1,0:T(8,128)(2,1)S(1)}, bf16[16,2048]{1,0:T(8,128)(2,1)}, u32[]{:S(2)}) copy-start(bf16[16,2048]{1,0:T(8,128)(2,1)} %param.20) | copy-start | bytes 196612
  3.8 2.4 %copy-start.11 = (bf16[2048,4]{0,1:T(4,128)(2,1)S(1)}, bf16[2048,4]{0,1:T(4,128)(2,1)}, u32[]{:S(2)}) copy-start(bf16[2048,4]{0,1:T(4,128)(2,1)} %param.25) | copy-start | bytes 49156
  3.9 2.7 %copy-start.1 = (f32[16,4,1024]{2,1,0:T(4,128)S(1)}, f32[16,4,1024]{2,1,0:T(4,128)}, u32[]{:S(2)}) copy-start(f32[16,4,1024]{2,1,0:T(4,128)} %param.29) | copy-start | bytes 786436
  3.9 3.0 %copy-start.3 = (bf16[2048,256]{1,0:T(8,128)(2,1)S(1)}, bf16[2048,256]{1,0:T(8,128)(2,1)}, u32[]{:S(2)}) copy-start(bf16[2048,256]{1,0:T(8,128)(2,1)} %param.22) | copy-start | bytes 3145732
  7.3 6.5 %copy-start.6 = (bf16[2048,128]{1,0:T(8,128)(2,1)S(1)}, bf16[2048,128]{1,0:T(8,128)(2,1)}, u32[]{:S(2)}) copy-start(bf16[2048,128]{1,0:T(8,128)(2,1)} %param.23) | copy-start | bytes 1572868
  13.8 3.9 %copy-start.7 = (bf16[2048,128]{1,0:T(8,128)(2,1)S(1)}, bf16[2048,128]{1,0:T(8,128)(2,1)}, u32[]{:S(2)}) copy-start(bf16[2048,128]{1,0:T(8,128)(2,1)} %param.24) | copy-start | bytes 1572868
  24.4 3.6 %copy-start.4 = (bf16[256,2048]{1,0:T(8,128)(2,1)S(1)}, bf16[256,2048]{1,0:T(8,128)(2,1)}, u32[]{:S(2)}) copy-start(bf16[256,2048]{1,0:T(8,128)(2,1)} %param.26) | copy-start | bytes 3145732
  24.4 7.1 %copy-start.10 = (bf16[2048]{0:T(1024)(128)(2,1)S(1)}, bf16[2048]{0:T(1024)(128)(2,1)}, u32[]{:S(2)}) copy-start(bf16[2048]{0:T(1024)(128)(2,1)} %param.31) | copy-start | bytes 12292
  28.0 18.8 %copy-start.8 = (s32[16,6]{0,1:T(8,128)S(1)}, s32[16,6]{0,1:T(8,128)}, u32[]{:S(2)}) copy-start(s32[16,6]{0,1:T(8,128)} %param.33) | copy-start | bytes 1156
  28.3 18.7 %copy-start.5 = (bf16[2048,256]{1,0:T(8,128)(2,1)S(1)}, bf16[2048,256]{1,0:T(8,128)(2,1)}, u32[]{:S(2)}) copy-start(bf16[2048,256]{1,0:T(8,128)(2,1)} %param.34) | copy-start | bytes 3145732
  35.3 29.4 %all-to-all-start.1 = ((bf16[64,3,2048]{2,1,0:T(4,128)(2,1)}), bf16[64,3,2048]{2,1,0:T(4,128)(2,1)}, u32[]{:S(2)}, u32[]{:S(2)}) async-start(bf16[64,3,2048]{2,1,0:T(4,128)(2,1)} %reshape.261), calls=%async_computation.1 | async-start | bytes 2097152 | tf_op jit(solution)/shard_map/all_to_all | solution.py:157
  77.2 6.4 %all-to-all-start = ((bf16[2,16,2048]{2,1,0:T(8,128)(2,1)}), bf16[2,16,2048]{2,1,0:T(8,128)(2,1)}, u32[]{:S(2)}, u32[]{:S(2)}) async-start(bf16[2,16,2048]{2,1,0:T(8,128)(2,1)} %broadcast_in_dim.79), calls=%async_computation | async-start | bytes 262144 | tf_op jit(solution)/shard_map/all_to_all | solution.py:20
  83.6 23.1 %all-to-all-start.3 = ((bf16[64,3,2048]{2,1,0:T(4,128)(2,1)}), bf16[64,3,2048]{2,1,0:T(4,128)(2,1)S(1)}, u32[]{:S(2)}, u32[]{:S(2)}) async-start(bf16[64,3,2048]{2,1,0:T(4,128)(2,1)} %copy.89), calls=%async_computation.3 | async-start | bytes 2097152 | tf_op jit(solution)/shard_map/all_to_all | solution.py:167
where the time goes:
time: 110 us; the launch traced here: 109 us
  waiting for transfers between devices  29.9 us (27%)
  local copies, waits for them, and re-layouts  25.8 us (23%)
  starting transfers between devices  20.5 us (19%)
  matrix products  16.8 us (15%)
  blocking collectives  9.44 us (9%)
  other arithmetic  6.55 us (6%)
    all_to_all x1, waiting for transfers between devices, per_device(): lax.all_to_all(outgoing, 'ep', split_axis=0, concat_axis=0, tiled=True)  15.2 us
    all_to_all x1, waiting for transfers between devices, per_device(): lax.all_to_all(merged, 'ep', split_axis=0, concat_axis=0, tiled=True)  14.7 us
    unnamed x29, local copies, waits for them, and re-layouts  13.7 us
    all_to_all x1, starting transfers between devices, per_device(): lax.all_to_all(outgoing, 'ep', split_axis=0, concat_axis=0, tiled=True)  11.5 us
    all_to_all x1, blocking collectives, copy_for_each(): lax.all_to_all(jnp.broadcast_to(array[None], (size, *array.shape)), axis,...  6.39 us
    all_to_all x1, starting transfers between devices, per_device(): lax.all_to_all(merged, 'ep', split_axis=0, concat_axis=0, tiled=True)  4.65 us
    all_to_all x1, starting transfers between devices, copy_for_each(): lax.all_to_all(jnp.broadcast_to(array[None], (size, *array.shape)), axis,...  4.36 us
    dot_general x1, matrix products, attend(): jnp.einsum('skgl,slkd->skgd', past_prob, cached_values, preferred_element...  3.52 us
  transfers between devices with their start and end apart: 3, of which 2 were waited for; matrix products, arithmetic and copies ran while one was open for 8% of the time, Pallas kernels for 0%

commit v1 on v0

v1 whole, which is shorter than its diff:
```python
import functools

import jax
import jax.numpy as jnp
from jax import lax
from jax.experimental import pallas as pl
from jax.experimental.pallas import tpu as pltpu
from jax.sharding import PartitionSpec as P

HEAD_DIM = 64
EPS = 1e-06
ROUTE_SCALE = 2.5
CAP = 3
MESH = pl.DeviceIdType.MESH
F32 = jnp.float32
BF16 = jnp.bfloat16
HIGH = lax.Precision.HIGHEST
NT = (((1,), (1,)), ((), ()))
TN = (((0,), (0,)), ((), ()))
NN = (((1,), (0,)), ((), ()))


def dot(left, right, dims=NN, precision=None):
    return lax.dot_general(left, right, dims, precision=precision, preferred_element_type=F32)


def iota(shape, dim):
    return lax.broadcasted_iota(jnp.int32, shape, dim)


def norm_rows(values, gain):
    factor = lax.rsqrt(jnp.mean(values * values, axis=-1, keepdims=True) + EPS)
    return (values * factor * gain.astype(F32)).astype(BF16)


def silu(x):
    return x / (1.0 + jnp.exp(-x))


def log2(n):
    assert n & (n - 1) == 0
    return n.bit_length() - 1


def kernel(
    dims,
    tokens, norm_gain, w_query, w_key, w_value, w_forget, w_out, cache_keys, cache_values,
    cache_gates, lengths, ffn_gain, router_w, routes, shared_gate, shared_up, shared_down,
    expert_gate, expert_up, expert_down,
    out,
    tok, gain1, wq, wk, wv, wf, wo, kc, vc, gt, lens, gain2, rw, rt, sg, su, sd,
    eg, eu, ed, scores, heads, mine, theirs, xs, hid, lay, box_out, box_in, ret_out, ret_in,
    fin_out, fin_in, result,
    in_sem, k_sem, v_sem, att_sem, wt_send, wt_recv, go_send, go_recv, back_send, back_recv,
    fin_sem,
):
    nz, ny, nx = dims
    n_ep = nz * ny * nx
    half = n_ep // 2
    hx = nx // 2
    seqs, width = tokens.shape
    positions = cache_keys.shape[1]
    top_k = routes.shape[0]
    cols = width // 128
    rows = half * CAP
    pairs = seqs // 2
    ep = lax.axis_index("ep")
    core = lax.axis_index("tp")
    z, y, x = ep // (ny * nx), (ep // nx) % ny, ep % nx

    def peer(i, forward):
        dz = i // (ny * hx)
        dy = (i // hx) % ny
        dx = 2 * (i % hx) + (dz + dy + core) % 2
        if forward:
            pz, py, px = (z + dz) % nz, (y + dy) % ny, (x + dx) % nx
        else:
            pz, py, px = (z + nz - dz) % nz, (y + ny - dy) % ny, (x + nx - dx) % nx
        return (pz * ny + py) * nx + px

    def remote(i):
        return jnp.logical_or(core == 1, i > 0)

    barrier = pltpu.get_barrier_semaphore()

    def greet(i, carry):
        @pl.when(remote(i))
        def _():
            pl.semaphore_signal(
                barrier, inc=1, device_id=(peer(i, True), core), device_id_type=MESH
            )
        return carry

    lax.fori_loop(0, half, greet, 0)
    pl.semaphore_signal(barrier, inc=1, device_id=(ep, 1 - core), device_id_type=MESH)

    loads = {}
    order = (
        ("tok", tokens, tok), ("gain1", norm_gain, gain1), ("wq", w_query, wq), ("wk", w_key, wk),
        ("wv", w_value, wv), ("wf", w_forget, wf), ("lens", lengths, lens),
        ("gt", cache_gates, gt),
    )
    later = (
        ("wo", w_out, wo), ("gain2", ffn_gain, gain2), ("rt", routes, rt),
        ("eg", expert_gate.at[0], eg.at[0]), ("eu", expert_up.at[0], eu.at[0]),
        ("ed", expert_down.at[0], ed.at[0]),
        ("sg", shared_gate, sg), ("su", shared_up, su), ("sd", shared_down, sd),
        ("rw", router_w, rw),
    )
    slot = 0

    def load(name, src, dst):
        nonlocal slot
        loads[name] = pltpu.make_async_copy(src, dst, in_sem.at[slot])
        loads[name].start()
        slot += 1

    def ready(*names):
        for name in names:
            loads[name].wait()

    for item in order:
        load(*item)
    k_loads = []
    v_loads = []
    for p in range(pairs):
        k_loads.append(pltpu.make_async_copy(
            cache_keys.at[pl.ds(2 * p, 2)], kc.at[pl.ds(2 * p, 2)], k_sem.at[p]))
        k_loads[-1].start()
    for p in range(pairs):
        v_loads.append(pltpu.make_async_copy(
            cache_values.at[pl.ds(2 * p, 2)], vc.at[pl.ds(2 * p, 2)], v_sem.at[p]))
        v_loads[-1].start()
    for item in later:
        load(*item)

    ready("tok", "gain1")
    normed = norm_rows(tok[...].astype(F32), gain1[...])
    ready("wq")
    query = (dot(normed, wq[...]).astype(BF16).astype(F32)) * (HEAD_DIM ** -0.5)
    ready("wk")
    key_new = dot(normed, wk[...]).astype(BF16)
    ready("wv")
    value_new = dot(normed, wv[...]).astype(BF16)
    ready("wf")
    forget = dot(normed, wf[...], NT)
    forget = jnp.minimum(forget, 0.0) - jnp.log1p(jnp.exp(-jnp.abs(forget)))

    lane = iota((seqs, 128), 1)
    low = lane < 64
    q0, q1 = query[:, :128], query[:, 128:]
    q_cat = jnp.concatenate([
        jnp.where(low, q0, 0.0),
        jnp.where(low, pltpu.roll(q0, 64, 1), 0.0),
        jnp.where(low, 0.0, pltpu.roll(q1, 64, 1)),
        jnp.where(low, 0.0, q1),
    ], axis=0).astype(BF16)
    n_rows = 4 * seqs
    perm_r, perm_c = iota((n_rows, n_rows), 0), iota((n_rows, n_rows), 1)
    perm = (perm_c == (perm_r & 3) * seqs + (perm_r >> 2)).astype(F32).astype(BF16)
    spread = iota((n_rows, seqs), 1) == (iota((n_rows, seqs), 0) >> 2)
    spread_f = spread.astype(F32)
    spread_b = spread_f.astype(BF16)
    q_rows = dot(perm, q_cat)
    k_rows = dot(spread_b, key_new)
    v_rows = dot(spread_b, value_new)
    self_score = jnp.sum(q_rows * k_rows, axis=1, keepdims=True)
    gate_rows = dot(spread_f, forget, precision=HIGH)
    gate_rows = jnp.sum(
        jnp.where(iota((n_rows, 4), 1) == (iota((n_rows, 4), 0) & 3), gate_rows, 0.0),
        axis=1, keepdims=True)
    q_rows = q_rows.astype(BF16)

    ready("lens", "gt")
    first = iota((8, 128), 0) < 4
    first_pos = iota((8, positions), 0) < 4
    pos = iota((8, positions), 1)
    for p in range(pairs):
        k_loads[p].wait()
        q8 = q_rows[8 * p:8 * p + 8, :]
        zero = jnp.zeros_like(q8)
        q_pair = jnp.concatenate(
            [jnp.where(first, q8, zero), jnp.where(first, zero, q8)], axis=1)
        k_pair = jnp.concatenate([kc[2 * p], kc[2 * p + 1]], axis=1)
        s = dot(q_pair, k_pair, NT)
        g = jnp.concatenate([gt[2 * p], gt[2 * p + 1]], axis=0)
        count = jnp.where(first_pos, lens[2 * p], lens[2 * p + 1])
        last = jnp.sum(jnp.where(pos == count - 1, g, 0.0), axis=1, keepdims=True)
        s = s + ((last + gate_rows[8 * p:8 * p + 8, :]) - g)
        scores[8 * p:8 * p + 8, :] = jnp.where(pos < count, s, -jnp.inf)
    s = scores[...]
    peak = jnp.maximum(jnp.max(s, axis=1, keepdims=True), self_score)
    weight = jnp.exp(s - peak)
    self_weight = jnp.exp(self_score - peak)
    total = jnp.sum(weight, axis=1, keepdims=True) + self_weight
    scores[...] = weight / total
    self_prob = (self_weight / total).astype(BF16).astype(F32)
    for p in range(pairs):
        v_loads[p].wait()
        prob = scores[8 * p:8 * p + 8, :].astype(BF16)
        v_pair = jnp.concatenate([vc[2 * p], vc[2 * p + 1]], axis=1)
        mixed = dot(prob, v_pair)
        heads[8 * p:8 * p + 8, :] = jnp.where(first, mixed[:, :128], mixed[:, 128:])
    mixed = heads[...] + self_prob * v_rows
    row_high = (iota((n_rows, 128), 0) & 2) > 0
    lane_high = iota((n_rows, 128), 1) >= 64
    mixed = jnp.where(row_high == lane_high, mixed, 0.0).astype(BF16)
    a_cat = dot(perm, mixed, TN)
    a0, a1 = a_cat[:seqs], a_cat[seqs:2 * seqs]
    a2, a3 = a_cat[2 * seqs:3 * seqs], a_cat[3 * seqs:]
    attn = jnp.concatenate(
        [a0 + pltpu.roll(a1, 64, 1), pltpu.roll(a2, 64, 1) + a3], axis=1).astype(BF16)
    ready("wo")
    mine[...] = dot(attn, wo[...]).astype(BF16)

    pl.semaphore_wait(barrier, half + core)

    sibling = (ep, 1 - core)
    swap = pltpu.make_async_remote_copy(
        mine, theirs, att_sem.at[0], att_sem.at[1], device_id=sibling, device_id_type=MESH)
    swap.start()
    ready("eg", "eu", "ed")
    pushes = [
        pltpu.make_async_remote_copy(
            buf.at[0], buf.at[1], wt_send.at[n], wt_recv.at[n], device_id=sibling,
            device_id_type=MESH)
        for n, buf in enumerate((eg, eu, ed))
    ]
    for push in pushes:
        push.start()

    ready("gain2", "rt")
    slot_id = iota((rows, 1), 0)
    magic = -(-4096 // CAP)
    assert all((l * magic) >> 12 == l // CAP for l in range(rows))
    peer_i = (slot_id * magic) >> 12
    rank_of = slot_id - peer_i * CAP
    lhx, lny, lnx = log2(hx), log2(ny), log2(nx)
    dz = peer_i >> (lny + lhx)
    dy = (peer_i >> lhx) & (ny - 1)
    dx = 2 * (peer_i & (hx - 1)) + ((dz + dy + core) & 1)
    expert_of = (
        (((z + dz) & (nz - 1)) << (lny + lnx)) + (((y + dy) & (ny - 1)) << lnx)
        + ((x + dx) & (nx - 1)))
    routed_to = rt[...]
    marks = jnp.zeros((rows, seqs), F32)
    marks_all = jnp.zeros((n_ep, seqs), F32)
    all_experts = iota((n_ep, seqs), 0)
    for k in range(top_k):
        marks = marks + (routed_to[k:k + 1, :] == expert_of).astype(F32)
        marks_all = marks_all + (routed_to[k:k + 1, :] == all_experts).astype(F32)
    earlier = (iota((seqs, seqs), 0) < iota((seqs, seqs), 1)).astype(F32)
    rank = dot(marks.astype(BF16), earlier.astype(BF16))
    pick = jnp.where(rank == rank_of.astype(F32), marks, 0.0)
    pick_b = pick.astype(BF16)

    swap.wait_recv()
    residual = (
        tok[...].astype(F32) + (mine[...].astype(F32) + theirs[...].astype(F32))).astype(BF16)
    ffn_rows = norm_rows(residual.astype(F32), gain2[...])

    for j in range(cols // 2):
        part = dot(pick_b, ffn_rows[:, 256 * j:256 * j + 256])
        lay[pl.ds(2 * j, rows, stride=cols), :] = part[:, :128]
        lay[pl.ds(2 * j + 1, rows, stride=cols), :] = part[:, 128:]
    box_out[...] = lay[...].astype(BF16).reshape(box_out.shape)

    def go(i):
        return pltpu.make_async_remote_copy(
            box_out.at[i], box_in.at[i], go_send.at[i], go_recv.at[i],
            device_id=(peer(i, True), core), device_id_type=MESH)

    def back(i):
        return pltpu.make_async_remote_copy(
            ret_out.at[i], ret_in.at[i], back_send.at[i], back_recv.at[i],
            device_id=(peer(i, False), core), device_id_type=MESH)

    def each(action):
        def step(i, carry):
            @pl.when(remote(i))
            def _():
                action(i)
            return carry
        lax.fori_loop(0, half, step, 0)

    each(lambda i: go(i).start())

    @pl.when(core == 0)
    def _():
        box_in[0] = box_out[0]

    ready("rw")
    chance = dot(rw[...], ffn_rows, NT)
    chance = marks_all / (1.0 + jnp.exp(-chance))
    share = ROUTE_SCALE * chance / jnp.sum(chance, axis=0, keepdims=True)
    to_slot = (iota((rows, n_ep), 1) == expert_of).astype(F32)
    slot_w = dot(to_slot, share, precision=HIGH) * pick
    slot_hi = slot_w.astype(BF16)
    slot_lo = (slot_w - slot_hi.astype(F32)).astype(BF16)
    ready("sg", "su", "sd")
    shared_h = (silu(dot(ffn_rows, sg[...])) * dot(ffn_rows, su[...])).astype(BF16)
    shared = dot(shared_h, sd[...]).astype(BF16)
    fin_out[...] = shared.astype(F32)

    each(lambda i: go(i).wait_recv())
    lay[...] = box_in[...].reshape(lay.shape).astype(F32)
    for j in range(cols):
        xs[:, 128 * j:128 * j + 128] = lay[pl.ds(j, rows, stride=cols), :].astype(BF16)
    hidden_w = eg.shape[2]
    for part in range(2):
        if part == 1:
            for push in pushes:
                push.wait_recv()
        gate = dot(xs[...], eg[part])
        up = dot(xs[...], eu[part])
        hid[:, hidden_w * part:hidden_w * (part + 1)] = (silu(gate) * up).astype(BF16)
    for j in range(cols // 2):
        down = ed[:, :, 256 * j:256 * j + 256].reshape(2 * hidden_w, 256)
        answer = dot(hid[...], down)
        lay[pl.ds(2 * j, rows, stride=cols), :] = answer[:, :128]
        lay[pl.ds(2 * j + 1, rows, stride=cols), :] = answer[:, 128:]
    ret_out[...] = lay[...].astype(BF16).reshape(ret_out.shape)
    each(lambda i: back(i).start())

    @pl.when(core == 0)
    def _():
        ret_in[0] = ret_out[0]

    each(lambda i: back(i).wait_recv())
    lay[...] = ret_in[...].reshape(lay.shape).astype(F32)
    for j in range(cols):
        answer = lay[pl.ds(j, rows, stride=cols), :].astype(BF16)
        part = dot(slot_hi, answer, TN) + dot(slot_lo, answer, TN)
        fin_out[:, 128 * j:128 * j + 128] += part

    finish = pltpu.make_async_remote_copy(
        fin_out, fin_in, fin_sem.at[0], fin_sem.at[1], device_id=sibling, device_id_type=MESH)
    finish.start()
    finish.wait_recv()
    result[...] = (residual.astype(F32) + (fin_out[...] + fin_in[...])).astype(BF16)
    write = pltpu.make_async_copy(result, out, in_sem.at[0])
    write.start()
    finish.wait_send()
    swap.wait_send()
    for push in pushes:
        push.wait_send()
    each(lambda i: go(i).wait_send())
    each(lambda i: back(i).wait_send())
    write.wait()


def split_dims(n):
    return {64: (4, 4, 4), 4: (1, 2, 2), 8: (2, 2, 2)}[n]


def per_device(
    tokens, norm_gain, w_query, w_key, w_value, w_forget, w_out, cache_keys, cache_values,
    cache_gates, lengths, ffn_gain, router_w, routes, shared_gate, shared_up, shared_down,
    expert_gate, expert_up, expert_down,
):
    seqs, width = tokens.shape
    n_ep = lax.axis_size("ep")
    half = n_ep // 2
    rows = half * CAP
    cols = width // 128
    positions = cache_keys.shape[1]
    ff = expert_gate.shape[2]
    any_spec = pl.BlockSpec(memory_space=pl.ANY)
    operands = (
        tokens, norm_gain.reshape(1, width), w_query, w_key, w_value, w_forget.T, w_out,
        cache_keys, cache_values, cache_gates, lengths, ffn_gain.reshape(1, width), router_w.T,
        routes.T, shared_gate, shared_up, shared_down, expert_gate, expert_up, expert_down,
    )
    vmem = pltpu.VMEM
    dma = pltpu.SemaphoreType.DMA

    def like(index):
        return vmem(operands[index].shape, operands[index].dtype)

    scratch = [
        like(0), like(1), like(2), like(3), like(4), like(5), like(6), like(7), like(8), like(9),
        pltpu.SMEM(lengths.shape, jnp.int32), like(11), like(12), like(13), like(14), like(15),
        like(16),
        vmem((2, width, ff), BF16), vmem((2, width, ff), BF16), vmem((2, ff, width), BF16),
        vmem((4 * seqs, positions), F32), vmem((4 * seqs, 128), F32),
        vmem((seqs, width), BF16), vmem((seqs, width), BF16),
        vmem((rows, width), BF16), vmem((rows, 2 * ff), BF16), vmem((rows * cols, 128), F32),
        vmem((half, CAP * cols, 128), BF16), vmem((half, CAP * cols, 128), BF16),
        vmem((half, CAP * cols, 128), BF16), vmem((half, CAP * cols, 128), BF16),
        vmem((seqs, width), F32), vmem((seqs, width), F32), vmem((seqs, width), BF16),
        dma((18,)), dma((seqs // 2,)), dma((seqs // 2,)), dma((2,)), dma((3,)), dma((3,)),
        dma((half,)), dma((half,)), dma((half,)), dma((half,)), dma((2,)),
    ]
    return pl.pallas_call(
        functools.partial(kernel, split_dims(n_ep)),
        out_shape=jax.ShapeDtypeStruct((seqs, width), BF16),
        in_specs=[any_spec] * len(operands),
        out_specs=any_spec,
        scratch_shapes=scratch,
        compiler_params=pltpu.CompilerParams(
            collective_id=0, has_side_effects=True, vmem_limit_bytes=62 * 1024 * 1024),
    )(*operands)


def solution(mesh):
    placed = (
        P("ep", None),
        P(),
        P(None, "tp"),
        P(None, "tp"),
        P(None, "tp"),
        P(None, "tp"),
        P("tp", None),
        P("ep", None, "tp"),
        P("ep", None, "tp"),
        P("ep", "tp", None),
        P("ep"),
        P(),
        P(),
        P("ep", None),
        P(None, "tp"),
        P(None, "tp"),
        P("tp", None),
        P("ep", None, "tp"),
        P("ep", None, "tp"),
        P("ep", "tp", None),
    )
    return jax.shard_map(
        per_device, mesh=mesh, in_specs=placed, out_specs=P("ep", None), check_vma=False
    )
```

time: 110 us -> 43.6 us (0.40)
  Pallas kernels: 0 us -> 39.3 us
  waiting for transfers between devices: 29.9 us -> 0 us
  local copies, waits for them, and re-layouts: 25.8 us -> 4.05 us
  starting transfers between devices: 20.5 us -> 0 us
  matrix products: 16.8 us -> 0 us
  blocking collectives: 9.44 us -> 0 us
  other arithmetic: 6.55 us -> 0 us
    pallas_call x0 -> x1, Pallas kernels: none -> 39.3 us  [per_device(): pl.pallas_call(functools.partial(kernel, split_dims(n_ep)), out_shape=jax...]
    all_to_all x3 -> x0, waiting for transfers between devices: 29.9 us -> none  [the longest x1 15.2 us: per_device(): lax.all_to_all(outgoing, 'ep', split_axis=0, concat_axis=0, tiled=True)]
    all_to_all x3 -> x0, starting transfers between devices: 20.5 us -> none  [the longest x1 11.5 us: per_device(): lax.all_to_all(outgoing, 'ep', split_axis=0, concat_axis=0, tiled=True)]
    dot_general x13 -> x0, matrix products: 16.8 us -> none  [the longest x1 3.52 us: attend(): jnp.einsum('skgl,slkd->skgd', past_prob, cached_values, preferred_element...]
    unnamed x29 -> x1, local copies, waits for them, and re-layouts: 13.7 us -> 1.47 us
    all_to_all x1 -> x0, blocking collectives: 6.39 us -> none  [copy_for_each(): lax.all_to_all(jnp.broadcast_to(array[None], (size, *array.shape)), axis,...]
    gather x11 -> x0, local copies, waits for them, and re-layouts: 4.84 us -> none  [the longest x5 2.38 us: attend(): last_gate = jnp.take_along_axis(cache_gates, last_index, axis=2)]
    all_gather x1 -> x0, blocking collectives: 3.05 us -> none  [total_of_pieces(): parts = lax.all_gather(array, axis).astype(jnp.float32)]
  transfers between devices with their start and end apart: 3 -> 0, of which waited for: 2 -> 0; matrix products, arithmetic and copies ran while one was open for 8% -> 0% of each run, Pallas kernels for 0% -> 0%
where the time goes in v1:
time: 43.6 us; the launch traced here: 43.4 us
  Pallas kernels  39.3 us (90%)
  local copies, waits for them, and re-layouts  4.05 us (9%)
    pallas_call x1, Pallas kernels, per_device(): pl.pallas_call(functools.partial(kernel, split_dims(n_ep)), out_shape=jax...  39.3 us
    unnamed x1, local copies, waits for them, and re-layouts  1.47 us
    reshape x1, local copies, waits for them, and re-layouts, per_device(): norm_gain.reshape(1, width)  1.29 us
    reshape x1, local copies, waits for them, and re-layouts, per_device(): ffn_gain.reshape(1, width)  1.28 us

profile of v1, /device:TPU:1, one launch (start us, length us, event | category | flops | bytes accessed | tf_op | source)
XLA Modules:
  0.0 43.4 jit_solution(1086459021377010185)
XLA Ops:
  0.0 1.3 %reshape.6.norm_gain = bf16[1,2048]{1,0:T(2,128)(2,1)} reshape(bf16[2048]{0:T(1024)(128)(2,1)} %param.21) | data formatting | bytes 8192 | tf_op jit(solution)/shard_map/reshape | solution.py:370
  1.3 1.3 %reshape.7.ffn_gain = bf16[1,2048]{1,0:T(2,128)(2,1)} reshape(bf16[2048]{0:T(1024)(128)(2,1)} %param.31) | data formatting | bytes 8192 | tf_op jit(solution)/shard_map/reshape | solution.py:371
  2.6 39.3 %shard_map.190 = bf16[16,2048]{1,0:T(8,128)(2,1)} custom-call(bf16[16,2048]{1,0:T(8,128)(2,1)} %tokens.1, bf16[1,2048]{1,0:T(2,128)(2,1)} %reshape.6.norm_gain, bf16[2048,256]{1,0:T(8,128)(2,1)} %w_query.1, bf16[2048,128]{1,0:T(8,128)(2,1)} %w_key.1, bf16[2048,128]{1,0:T(8,128)(2,1)} %w_value.1, bf16[4,2048]{1,0:T(4,128)(2,1)} %bitcast.4, ...), custom_call_target="tpu_custom_call" | custom-call | tf_op jit(solution)/shard_map/pallas_call | solution.py:394
  41.9 1.5 %copy.22 = bf16[16,2048]{1,0:T(8,128)(2,1)} copy(bf16[16,2048]{1,0:T(8,128)(2,1)} %shard_map.190) | data formatting | bytes 131072

commit v2 on v1

v2 whole, which is shorter than its diff:
```python
import functools

import jax
import jax.numpy as jnp
from jax import lax
from jax.experimental import pallas as pl
from jax.experimental.pallas import tpu as pltpu
from jax.sharding import PartitionSpec as P

HEAD_DIM = 64
EPS = 1e-06
ROUTE_SCALE = 2.5
CAP = 3
GROUPS = 2
MESH = pl.DeviceIdType.MESH
F32 = jnp.float32
BF16 = jnp.bfloat16
HIGH = lax.Precision.HIGHEST
NT = (((1,), (1,)), ((), ()))
TN = (((0,), (0,)), ((), ()))
NN = (((1,), (0,)), ((), ()))


def dot(left, right, dims=NN, precision=None):
    return lax.dot_general(left, right, dims, precision=precision, preferred_element_type=F32)


def iota(shape, dim):
    return lax.broadcasted_iota(jnp.int32, shape, dim)


def norm_rows(values, gain):
    factor = lax.rsqrt(jnp.mean(values * values, axis=-1, keepdims=True) + EPS)
    return (values * factor * gain.astype(F32)).astype(BF16)


def silu(x):
    return x / (1.0 + jnp.exp(-x))


class Phases:
    def __init__(self):
        self.scope = None

    def __call__(self, name=None):
        if self.scope is not None:
            self.scope.__exit__(None, None, None)
        self.scope = jax.named_scope(name) if name else None
        if self.scope is not None:
            self.scope.__enter__()


def peer_tables(dims):
    nz, ny, nx = dims
    tables = ([], [])
    for dz in range(nz):
        for dy in range(ny):
            for dx in range(nx):
                far = min(dz, nz - dz) + min(dy, ny - dy) + min(dx, nx - dx)
                tables[dx % 2].append((-far, dz, dy, dx))
    return [[entry[1:] for entry in sorted(table)] for table in tables]


def log2(n):
    assert n & (n - 1) == 0
    return n.bit_length() - 1


def kernel(
    dims,
    tokens, norm_gain, w_query, w_key, w_value, w_forget, w_out, cache_keys, cache_values,
    cache_gates, lengths, ffn_gain, router_w, routes, shared_gate, shared_up, shared_down,
    expert_gate, expert_up, expert_down,
    out,
    tok, gain1, wq, wk, wv, wf, wo, kc, vc, gt, lens, gain2, rw, rt, sg, su, sd,
    eg, eu, ed, scores, heads, mine, theirs, xs, hid, lay, box_out, box_in, ret_out, ret_in,
    total_rows, fin_out, fin_in,
    in_sem, k_sem, v_sem, att_sem, wt_send, wt_recv, go_send, go_recv, back_send, back_recv,
    fin_sem,
):
    nz, ny, nx = dims
    n_ep = nz * ny * nx
    half = n_ep // 2
    group = half // GROUPS
    seqs, width = tokens.shape
    positions = cache_keys.shape[1]
    top_k = routes.shape[0]
    cols = width // 128
    rows = half * CAP
    g_rows = group * CAP
    pairs = seqs // 2
    ep = lax.axis_index("ep")
    core = lax.axis_index("tp")
    z, y, x = ep // (ny * nx), (ep // nx) % ny, ep % nx
    tables = peer_tables(dims)

    def by_core(first, second):
        return first if first == second else first + core * (second - first)

    def peer(i, forward):
        dz, dy, dx = (by_core(a, b) for a, b in zip(tables[0][i], tables[1][i]))
        if forward:
            pz, py, px = (z + dz) % nz, (y + dy) % ny, (x + dx) % nx
        else:
            pz, py, px = (z + nz - dz) % nz, (y + ny - dy) % ny, (x + nx - dx) % nx
        return (pz * ny + py) * nx + px

    def each(numbers, action):
        for i in numbers:
            if i < half - 1:
                action(i)
            else:
                pl.when(core == 1)(functools.partial(action, i))

    phase = Phases()
    phase("loads")
    loads = {}
    order = (
        ("tok", tokens, tok), ("gain1", norm_gain, gain1), ("wq", w_query, wq), ("wk", w_key, wk),
        ("wv", w_value, wv), ("wf", w_forget, wf), ("lens", lengths, lens),
        ("rt", routes, rt), ("gt", cache_gates, gt),
    )
    later = (
        ("wo", w_out, wo), ("gain2", ffn_gain, gain2),
        ("eg", expert_gate.at[0], eg.at[0]), ("eu", expert_up.at[0], eu.at[0]),
        ("ed", expert_down.at[0], ed.at[0]),
        ("sg", shared_gate, sg), ("su", shared_up, su), ("sd", shared_down, sd),
        ("rw", router_w, rw),
    )
    slot = 0

    def load(name, src, dst):
        nonlocal slot
        loads[name] = pltpu.make_async_copy(src, dst, in_sem.at[slot])
        loads[name].start()
        slot += 1

    def ready(*names):
        for name in names:
            loads[name].wait()

    for item in order:
        load(*item)
    k_loads = [
        pltpu.make_async_copy(
            cache_keys.at[pl.ds(2 * p, 2)], kc.at[pl.ds(2 * p, 2)], k_sem.at[p])
        for p in range(pairs)
    ]
    v_loads = [
        pltpu.make_async_copy(
            cache_values.at[pl.ds(2 * p, 2)], vc.at[pl.ds(2 * p, 2)], v_sem.at[p])
        for p in range(pairs)
    ]
    for p in range(pairs // 2):
        k_loads[p].start()

    phase("greet")
    barrier = pltpu.get_barrier_semaphore()

    def greet(i):
        pl.semaphore_signal(
            barrier, inc=1, device_id=(peer(i, True), core), device_id_type=MESH)

    each(range(half), greet)
    pl.semaphore_signal(barrier, inc=1, device_id=(ep, 1 - core), device_id_type=MESH)

    phase("slots")
    ready("rt")
    slot_id = iota((rows, 1), 0)
    magic = -(-4096 // CAP)
    assert all((l * magic) >> 12 == l // CAP for l in range(rows))
    peer_i = (slot_id * magic) >> 12
    rank_of = slot_id - peer_i * CAP
    lny, lnx = log2(ny), log2(nx)

    def packed(entry):
        return (entry[0] << (lny + lnx)) + (entry[1] << lnx) + entry[2]

    code = jnp.zeros_like(slot_id)
    for i in range(half):
        code = jnp.where(
            peer_i == i, by_core(packed(tables[0][i]), packed(tables[1][i])), code)
    dz, dy, dx = code >> (lny + lnx), (code >> lnx) & (ny - 1), code & (nx - 1)
    expert_of = (
        (((z + dz) & (nz - 1)) << (lny + lnx)) + (((y + dy) & (ny - 1)) << lnx)
        + ((x + dx) & (nx - 1)))
    routed_to = rt[...]
    marks = jnp.zeros((rows, seqs), F32)
    marks_all = jnp.zeros((n_ep, seqs), F32)
    all_experts = iota((n_ep, seqs), 0)
    for k in range(top_k):
        marks = marks + (routed_to[k:k + 1, :] == expert_of).astype(F32)
        marks_all = marks_all + (routed_to[k:k + 1, :] == all_experts).astype(F32)
    earlier = (iota((seqs, seqs), 0) < iota((seqs, seqs), 1)).astype(F32)
    rank = dot(marks.astype(BF16), earlier.astype(BF16))
    pick = jnp.where(rank == rank_of.astype(F32), marks, 0.0)
    pick_b = pick.astype(BF16)
    to_slot = (iota((rows, n_ep), 1) == expert_of).astype(F32)

    phase("project")
    ready("tok", "gain1")
    for p in range(pairs // 2, pairs):
        k_loads[p].start()
    normed = norm_rows(tok[...].astype(F32), gain1[...].reshape(1, width))
    ready("wq")
    query = (dot(normed, wq[...]).astype(BF16).astype(F32)) * (HEAD_DIM ** -0.5)
    ready("wk")
    key_new = dot(normed, wk[...]).astype(BF16)
    ready("wv")
    value_new = dot(normed, wv[...]).astype(BF16)
    ready("wf")
    forget = dot(normed, wf[...], NT)
    forget = jnp.minimum(forget, 0.0) - jnp.log1p(jnp.exp(-jnp.abs(forget)))

    lane = iota((seqs, 128), 1)
    low = lane < 64
    q0, q1 = query[:, :128], query[:, 128:]
    q_cat = jnp.concatenate([
        jnp.where(low, q0, 0.0),
        jnp.where(low, pltpu.roll(q0, 64, 1), 0.0),
        jnp.where(low, 0.0, pltpu.roll(q1, 64, 1)),
        jnp.where(low, 0.0, q1),
    ], axis=0).astype(BF16)
    n_rows = 4 * seqs
    perm_r, perm_c = iota((n_rows, n_rows), 0), iota((n_rows, n_rows), 1)
    perm = (perm_c == (perm_r & 3) * seqs + (perm_r >> 2)).astype(F32).astype(BF16)
    spread = iota((n_rows, seqs), 1) == (iota((n_rows, seqs), 0) >> 2)
    spread_f = spread.astype(F32)
    spread_b = spread_f.astype(BF16)
    q_rows = dot(perm, q_cat)
    k_rows = dot(spread_b, key_new)
    v_rows = dot(spread_b, value_new)
    self_score = jnp.sum(q_rows * k_rows, axis=1, keepdims=True)
    gate_rows = dot(spread_f, forget, precision=HIGH)
    gate_rows = jnp.sum(
        jnp.where(iota((n_rows, 4), 1) == (iota((n_rows, 4), 0) & 3), gate_rows, 0.0),
        axis=1, keepdims=True)
    q_rows = q_rows.astype(BF16)

    phase("score")
    phase("k_wait")
    for p in range(pairs):
        k_loads[p].wait()
        v_loads[p].start()
    phase("score2")
    ready("lens", "gt")
    first = iota((8, 128), 0) < 4
    first_pos = iota((8, positions), 0) < 4
    pos = iota((8, positions), 1)
    for p in range(pairs):
        q8 = q_rows[8 * p:8 * p + 8, :]
        zero = jnp.zeros_like(q8)
        q_pair = jnp.concatenate(
            [jnp.where(first, q8, zero), jnp.where(first, zero, q8)], axis=1)
        k_pair = jnp.concatenate([kc[2 * p], kc[2 * p + 1]], axis=1)
        s = dot(q_pair, k_pair, NT)
        g = jnp.concatenate([gt[2 * p], gt[2 * p + 1]], axis=0)
        count = jnp.where(first_pos, lens[2 * p], lens[2 * p + 1])
        last = jnp.sum(jnp.where(pos == count - 1, g, 0.0), axis=1, keepdims=True)
        s = s + ((last + gate_rows[8 * p:8 * p + 8, :]) - g)
        scores[8 * p:8 * p + 8, :] = jnp.where(pos < count, s, -jnp.inf)
    phase("softmax")
    s = scores[...]
    peak = jnp.maximum(jnp.max(s, axis=1, keepdims=True), self_score)
    weight = jnp.exp(s - peak)
    self_weight = jnp.exp(self_score - peak)
    total = jnp.sum(weight, axis=1, keepdims=True) + self_weight
    scores[...] = weight / total
    self_prob = (self_weight / total).astype(BF16).astype(F32)
    phase("values")
    for item in later:
        load(*item)
    phase("v_wait")
    for p in range(pairs):
        v_loads[p].wait()
    phase("values2")
    for p in range(pairs):
        prob = scores[8 * p:8 * p + 8, :].astype(BF16)
        v_pair = jnp.concatenate([vc[2 * p], vc[2 * p + 1]], axis=1)
        mixed = dot(prob, v_pair)
        heads[8 * p:8 * p + 8, :] = jnp.where(first, mixed[:, :128], mixed[:, 128:])
    mixed = heads[...] + self_prob * v_rows
    row_high = (iota((n_rows, 128), 0) & 2) > 0
    lane_high = iota((n_rows, 128), 1) >= 64
    mixed = jnp.where(row_high == lane_high, mixed, 0.0).astype(BF16)
    a_cat = dot(perm, mixed, TN)
    a0, a1 = a_cat[:seqs], a_cat[seqs:2 * seqs]
    a2, a3 = a_cat[2 * seqs:3 * seqs], a_cat[3 * seqs:]
    attn = jnp.concatenate(
        [a0 + pltpu.roll(a1, 64, 1), pltpu.roll(a2, 64, 1) + a3], axis=1).astype(BF16)
    ready("wo")
    mine[...] = dot(attn, wo[...]).astype(BF16)

    phase("barrier")
    pl.semaphore_wait(barrier, half + core)

    phase("swap_start")
    sibling = (ep, 1 - core)
    swap = pltpu.make_async_remote_copy(
        mine, theirs, att_sem.at[0], att_sem.at[1], device_id=sibling, device_id_type=MESH)
    swap.start()
    ready("gain2")
    phase("swap_wait")
    swap.wait_recv()
    phase("norm2")
    residual = (
        tok[...].astype(F32) + (mine[...].astype(F32) + theirs[...].astype(F32))).astype(BF16)
    ffn_rows = norm_rows(residual.astype(F32), gain2[...].reshape(1, width))

    phase("pack")

    def go(i):
        return pltpu.make_async_remote_copy(
            box_out.at[i], box_in.at[i], go_send.at[i], go_recv.at[i],
            device_id=(peer(i, True), core), device_id_type=MESH)

    def back(i):
        return pltpu.make_async_remote_copy(
            ret_out.at[i], ret_in.at[i], back_send.at[i], back_recv.at[i],
            device_id=(peer(i, False), core), device_id_type=MESH)

    def members(g):
        return range(g * group, (g + 1) * group)

    def lines(g, j):
        return pl.ds(g * g_rows * cols + j, g_rows, stride=cols)

    def whole(g):
        return pl.ds(g * g_rows * cols, g_rows * cols)

    for g in range(GROUPS):
        chosen = pick_b[g * g_rows:(g + 1) * g_rows]
        for j in range(cols // 2):
            part = dot(chosen, ffn_rows[:, 256 * j:256 * j + 256])
            lay[lines(g, 2 * j), :] = part[:, :128]
            lay[lines(g, 2 * j + 1), :] = part[:, 128:]
        box_out[pl.ds(g * group, group)] = lay[whole(g), :].astype(BF16).reshape(
            group, CAP * cols, 128)
        each(members(g), lambda i: go(i).start())

    @pl.when(core == 0)
    def _():
        box_in[half - 1] = box_out[half - 1]

    ready("eg", "eu", "ed")
    pushes = [
        pltpu.make_async_remote_copy(
            buf.at[0], buf.at[1], wt_send.at[n], wt_recv.at[n], device_id=sibling,
            device_id_type=MESH)
        for n, buf in enumerate((eg, eu, ed))
    ]
    for push in pushes:
        push.start()

    phase("shared")
    ready("rw")
    chance = dot(rw[...], ffn_rows, NT)
    chance = marks_all / (1.0 + jnp.exp(-chance))
    share = ROUTE_SCALE * chance / jnp.sum(chance, axis=0, keepdims=True)
    slot_w = dot(to_slot, share, precision=HIGH) * pick
    slot_hi = slot_w.astype(BF16).astype(F32)
    slot_w = jnp.concatenate([slot_hi, slot_w - slot_hi], axis=1)
    mix = [
        jnp.transpose(slot_w[g * g_rows:(g + 1) * g_rows]).astype(BF16) for g in range(GROUPS)
    ]
    ready("sg", "su", "sd")
    shared_h = (silu(dot(ffn_rows, sg[...])) * dot(ffn_rows, su[...])).astype(BF16)
    total_rows[...] = dot(shared_h, sd[...])

    hidden_w = eg.shape[2]
    for g in range(GROUPS):
        phase(f"go_wait{g}")
        each(members(g), lambda i: go(i).wait_recv())
        phase(f"unpack{g}")
        lay[whole(g), :] = box_in[pl.ds(g * group, group)].reshape(
            g_rows * cols, 128).astype(F32)
        for j in range(cols):
            xs[:, 128 * j:128 * j + 128] = lay[lines(g, j), :].astype(BF16)
        phase(f"ffn_in{g}")
        for part in range(2):
            if part == 1 and g == 0:
                for push in pushes:
                    push.wait_recv()
            gate = dot(xs[...], eg[part])
            up = dot(xs[...], eu[part])
            hid[:, hidden_w * part:hidden_w * (part + 1)] = (silu(gate) * up).astype(BF16)
        phase(f"ffn_out{g}")
        for j in range(cols // 2):
            down = ed[:, :, 256 * j:256 * j + 256].reshape(2 * hidden_w, 256)
            answer = dot(hid[...], down)
            lay[lines(g, 2 * j), :] = answer[:, :128]
            lay[lines(g, 2 * j + 1), :] = answer[:, 128:]
        ret_out[pl.ds(g * group, group)] = lay[whole(g), :].astype(BF16).reshape(
            group, CAP * cols, 128)
        phase(f"back_start{g}")
        each(members(g), lambda i: back(i).start())

    @pl.when(core == 0)
    def _():
        ret_in[half - 1] = ret_out[half - 1]

    for g in range(GROUPS):
        phase(f"back_wait{g}")
        each(members(g), lambda i: back(i).wait_recv())
        phase(f"combine{g}")
        lay[whole(g), :] = ret_in[pl.ds(g * group, group)].reshape(
            g_rows * cols, 128).astype(F32)
        for j in range(cols // 2):
            answer = jnp.concatenate(
                [lay[lines(g, 2 * j), :], lay[lines(g, 2 * j + 1), :]], axis=1).astype(BF16)
            part = dot(mix[g], answer)
            part = total_rows[:, 256 * j:256 * j + 256] + (part[:seqs] + part[seqs:])
            if g < GROUPS - 1:
                total_rows[:, 256 * j:256 * j + 256] = part
            else:
                fin_out[:, 256 * j:256 * j + 256] = part.astype(BF16)

    phase("finish")
    finish = pltpu.make_async_remote_copy(
        fin_out, fin_in, fin_sem.at[0], fin_sem.at[1], device_id=sibling, device_id_type=MESH)
    finish.start()
    swap.wait_send()
    for push in pushes:
        push.wait_send()
    each(range(half), lambda i: go(i).wait_send())
    each(range(half), lambda i: back(i).wait_send())
    finish.wait_recv()
    phase("result")
    out[...] = (
        residual.astype(F32) + (fin_out[...].astype(F32) + fin_in[...].astype(F32))).astype(BF16)
    finish.wait_send()
    phase()


def split_dims(n):
    return {64: (4, 4, 4), 4: (1, 2, 2), 8: (2, 2, 2)}[n]


def per_device(
    tokens, norm_gain, w_query, w_key, w_value, w_forget, w_out, cache_keys, cache_values,
    cache_gates, lengths, ffn_gain, router_w, routes, shared_gate, shared_up, shared_down,
    expert_gate, expert_up, expert_down,
):
    seqs, width = tokens.shape
    n_ep = lax.axis_size("ep")
    half = n_ep // 2
    rows = half * CAP
    cols = width // 128
    positions = cache_keys.shape[1]
    ff = expert_gate.shape[2]
    any_spec = pl.BlockSpec(memory_space=pl.ANY)
    operands = (
        tokens, norm_gain, w_query, w_key, w_value, w_forget.T, w_out,
        cache_keys, cache_values, cache_gates, lengths, ffn_gain, router_w.T,
        routes.T, shared_gate, shared_up, shared_down, expert_gate, expert_up, expert_down,
    )
    vmem = pltpu.VMEM
    dma = pltpu.SemaphoreType.DMA

    def like(index):
        return vmem(operands[index].shape, operands[index].dtype)

    scratch = [
        like(0), like(1), like(2), like(3), like(4), like(5), like(6), like(7), like(8), like(9),
        pltpu.SMEM(lengths.shape, jnp.int32), like(11), like(12), like(13), like(14), like(15),
        like(16),
        vmem((2, width, ff), BF16), vmem((2, width, ff), BF16), vmem((2, ff, width), BF16),
        vmem((4 * seqs, positions), F32), vmem((4 * seqs, 128), F32),
        vmem((seqs, width), BF16), vmem((seqs, width), BF16),
        vmem((rows // GROUPS, width), BF16), vmem((rows // GROUPS, 2 * ff), BF16), vmem((rows * cols, 128), F32),
        vmem((half, CAP * cols, 128), BF16), vmem((half, CAP * cols, 128), BF16),
        vmem((half, CAP * cols, 128), BF16), vmem((half, CAP * cols, 128), BF16),
        vmem((seqs, width), F32), vmem((seqs, width), BF16), vmem((seqs, width), BF16),
        dma((18,)), dma((seqs // 2,)), dma((seqs // 2,)), dma((2,)), dma((3,)), dma((3,)),
        dma((half,)), dma((half,)), dma((half,)), dma((half,)), dma((2,)),
    ]
    return pl.pallas_call(
        functools.partial(kernel, split_dims(n_ep)),
        out_shape=jax.ShapeDtypeStruct((seqs, width), BF16),
        in_specs=[any_spec] * len(operands),
        out_specs=pl.BlockSpec(memory_space=pltpu.VMEM),
        scratch_shapes=scratch,
        compiler_params=pltpu.CompilerParams(
            collective_id=0, has_side_effects=True, vmem_limit_bytes=62 * 1024 * 1024),
    )(*operands)


def solution(mesh):
    placed = (
        P("ep", None),
        P(),
        P(None, "tp"),
        P(None, "tp"),
        P(None, "tp"),
        P(None, "tp"),
        P("tp", None),
        P("ep", None, "tp"),
        P("ep", None, "tp"),
        P("ep", "tp", None),
        P("ep"),
        P(),
        P(),
        P("ep", None),
        P(None, "tp"),
        P(None, "tp"),
        P("tp", None),
        P("ep", None, "tp"),
        P("ep", None, "tp"),
        P("ep", "tp", None),
    )
    return jax.shard_map(
        per_device, mesh=mesh, in_specs=placed, out_specs=P("ep", None), check_vma=False
    )
```

time: 43.6 us -> 34.8 us (0.80)
  Pallas kernels: 39.3 us -> 33.1 us
  local copies, waits for them, and re-layouts: 4.05 us -> 1.47 us
    pallas_call x1, Pallas kernels: 39.3 us -> 33.1 us  [per_device(): pl.pallas_call(functools.partial(kernel, split_dims(n_ep)), out_shape=jax...]
    reshape x2 -> x0, local copies, waits for them, and re-layouts: 2.57 us -> none  [the longest x1 1.29 us: per_device(): norm_gain.reshape(1, width)]
where the time goes in v2:
time: 34.8 us; the launch traced here: 34.6 us
  Pallas kernels  33.1 us (95%)
  local copies, waits for them, and re-layouts  1.47 us (4%)
    pallas_call x1, Pallas kernels, per_device(): pl.pallas_call(functools.partial(kernel, split_dims(n_ep)), out_shape=jax...  33.1 us
    unnamed x1, local copies, waits for them, and re-layouts  1.47 us

profile of v2, /device:TPU:1, one launch (start us, length us, event | category | flops | bytes accessed | tf_op | source)
XLA Modules:
  0.0 34.6 jit_solution(15461289086100591536)
XLA Ops:
  0.0 33.1 %shard_map.190 = bf16[16,2048]{1,0:T(8,128)(2,1)} custom-call(bf16[16,2048]{1,0:T(8,128)(2,1)} %tokens.1, bf16[2048]{0:T(1024)(128)(2,1)} %norm_gain.1, bf16[2048,256]{1,0:T(8,128)(2,1)} %w_query.1, bf16[2048,128]{1,0:T(8,128)(2,1)} %w_key.1, bf16[2048,128]{1,0:T(8,128)(2,1)} %w_value.1, bf16[4,2048]{1,0:T(4,128)(2,1)} %bitcast.4, bf16[256,2048]{1,0:T(8,128)(2,1)} %w_out.1, ...), custom_call_target="tpu_custom_call" | custom-call | tf_op jit(solution)/shard_map/pallas_call | solution.py:477
  33.1 1.5 %copy.22 = bf16[16,2048]{1,0:T(8,128)(2,1)} copy(bf16[16,2048]{1,0:T(8,128)(2,1)} %shard_map.190) | data formatting | bytes 131072

commit v3 on v2

--- a/solution.py
+++ b/solution.py
@@ -12,6 +12,9 @@
 ROUTE_SCALE = 2.5
 CAP = 3
 GROUPS = 2
+SLOTS = 9
+SPLIT = 4
+FAR_TURNS = {5: (1,), 4: (1, 1, 0), 1: (0,)}
 MESH = pl.DeviceIdType.MESH
 F32 = jnp.float32
 BF16 = jnp.bfloat16
@@ -52,13 +55,33 @@
 
 def peer_tables(dims):
     nz, ny, nx = dims
-    tables = ([], [])
-    for dz in range(nz):
-        for dy in range(ny):
-            for dx in range(nx):
-                far = min(dz, nz - dz) + min(dy, ny - dy) + min(dx, nx - dx)
-                tables[dx % 2].append((-far, dz, dy, dx))
-    return [[entry[1:] for entry in sorted(table)] for table in tables]
+
+    def far(entry):
+        return sum(min(d, n - d) for d, n in zip(entry, dims))
+
+    def negative(entry):
+        return tuple((n - d) % n for d, n in zip(entry, dims))
+
+    entries = [(dz, dy, dx) for dz in range(nz) for dy in range(ny) for dx in range(nx)]
+    half = len(entries) // 2
+    entries = sorted(entries[1:], key=lambda entry: (-far(entry), sum(entry), entry))
+    tables = ([(0, 0, 0)], [])
+    seen = {}
+    for entry in entries:
+        pair = sorted({entry, negative(entry)})
+        if len(pair) == 2 and entry == pair[0]:
+            count = seen.get(far(entry), 0)
+            seen[far(entry)] = count + 1
+            turns = FAR_TURNS.get(far(entry), (0, 1))
+            core = turns[count % len(turns)]
+            tables[core].extend(pair)
+    for entry in entries:
+        if entry == negative(entry):
+            tables[int(len(tables[1]) < half)].append(entry)
+    for table in tables:
+        table.sort(key=lambda entry: -far(entry))
+    assert len(tables[0]) == len(tables[1])
+    return tables
 
 
 def log2(n):
@@ -71,10 +94,10 @@
     tokens, norm_gain, w_query, w_key, w_value, w_forget, w_out, cache_keys, cache_values,
     cache_gates, lengths, ffn_gain, router_w, routes, shared_gate, shared_up, shared_down,
     expert_gate, expert_up, expert_down,
-    out,
+    out_residual, out_mine, out_theirs,
     tok, gain1, wq, wk, wv, wf, wo, kc, vc, gt, lens, gain2, rw, rt, sg, su, sd,
-    eg, eu, ed, scores, heads, mine, theirs, xs, hid, lay, box_out, box_in, ret_out, ret_in,
-    total_rows, fin_out, fin_in,
+    eg, eu, ed, scores, heads, fanned, mine, theirs, kept, xs, hid, lay, box_out, box_in, ret_out, ret_in,
+    total_rows, fin_out,
     in_sem, k_sem, v_sem, att_sem, wt_send, wt_recv, go_send, go_recv, back_send, back_recv,
     fin_sem,
 ):
@@ -116,22 +139,21 @@
     phase("loads")
     loads = {}
     order = (
-        ("tok", tokens, tok), ("gain1", norm_gain, gain1), ("wq", w_query, wq), ("wk", w_key, wk),
-        ("wv", w_value, wv), ("wf", w_forget, wf), ("lens", lengths, lens),
-        ("rt", routes, rt), ("gt", cache_gates, gt),
+        ("rt", routes, rt), ("tok", tokens, tok), ("gain1", norm_gain, gain1),
+        ("lens", lengths, lens), ("wf", w_forget, wf), ("wq", w_query, wq), ("wk", w_key, wk),
+        ("wv", w_value, wv), ("gt", cache_gates, gt),
     )
     later = (
-        ("wo", w_out, wo), ("gain2", ffn_gain, gain2),
+        ("rw", router_w, rw), ("gain2", ffn_gain, gain2),
         ("eg", expert_gate.at[0], eg.at[0]), ("eu", expert_up.at[0], eu.at[0]),
         ("ed", expert_down.at[0], ed.at[0]),
         ("sg", shared_gate, sg), ("su", shared_up, su), ("sd", shared_down, sd),
-        ("rw", router_w, rw),
     )
     slot = 0
 
     def load(name, src, dst):
         nonlocal slot
-        loads[name] = pltpu.make_async_copy(src, dst, in_sem.at[slot])
+        loads[name] = pltpu.make_async_copy(src, dst, in_sem.at[slot % SLOTS])
         loads[name].start()
         slot += 1
 
@@ -141,18 +163,16 @@
 
     for item in order:
         load(*item)
-    k_loads = [
-        pltpu.make_async_copy(
-            cache_keys.at[pl.ds(2 * p, 2)], kc.at[pl.ds(2 * p, 2)], k_sem.at[p])
-        for p in range(pairs)
-    ]
-    v_loads = [
-        pltpu.make_async_copy(
-            cache_values.at[pl.ds(2 * p, 2)], vc.at[pl.ds(2 * p, 2)], v_sem.at[p])
-        for p in range(pairs)
-    ]
-    for p in range(pairs // 2):
-        k_loads[p].start()
+    step = seqs // SPLIT
+
+    def cache_copy(src, dst, sem, n):
+        return pltpu.make_async_copy(
+            src.at[pl.ds(n * step, step)], dst.at[pl.ds(n * step, step)], sem.at[n])
+
+    k_loads = [cache_copy(cache_keys, kc, k_sem, n) for n in range(SPLIT)]
+    v_loads = [cache_copy(cache_values, vc, v_sem, n) for n in range(SPLIT)]
+    for copy in k_loads:
+        copy.start()
 
     phase("greet")
     barrier = pltpu.get_barrier_semaphore()
@@ -198,56 +218,52 @@
     to_slot = (iota((rows, n_ep), 1) == expert_of).astype(F32)
 
     phase("project")
-    ready("tok", "gain1")
-    for p in range(pairs // 2, pairs):
-        k_loads[p].start()
+    ready("tok", "gain1", "wq", "wk", "wv", "wf", "lens", "gt")
+    for copy in v_loads[:SPLIT // 2]:
+        copy.start()
     normed = norm_rows(tok[...].astype(F32), gain1[...].reshape(1, width))
-    ready("wq")
     query = (dot(normed, wq[...]).astype(BF16).astype(F32)) * (HEAD_DIM ** -0.5)
-    ready("wk")
-    key_new = dot(normed, wk[...]).astype(BF16)
-    ready("wv")
-    value_new = dot(normed, wv[...]).astype(BF16)
-    ready("wf")
+    key_new = dot(normed, wk[...]).astype(BF16).astype(F32)
+    value_new = dot(normed, wv[...]).astype(BF16).astype(F32)
     forget = dot(normed, wf[...], NT)
     forget = jnp.minimum(forget, 0.0) - jnp.log1p(jnp.exp(-jnp.abs(forget)))
 
-    lane = iota((seqs, 128), 1)
-    low = lane < 64
+    n_rows = 4 * seqs
+    low = iota((seqs, 128), 1) < 64
     q0, q1 = query[:, :128], query[:, 128:]
-    q_cat = jnp.concatenate([
-        jnp.where(low, q0, 0.0),
-        jnp.where(low, pltpu.roll(q0, 64, 1), 0.0),
-        jnp.where(low, 0.0, pltpu.roll(q1, 64, 1)),
-        jnp.where(low, 0.0, q1),
-    ], axis=0).astype(BF16)
-    n_rows = 4 * seqs
-    perm_r, perm_c = iota((n_rows, n_rows), 0), iota((n_rows, n_rows), 1)
-    perm = (perm_c == (perm_r & 3) * seqs + (perm_r >> 2)).astype(F32).astype(BF16)
-    spread = iota((n_rows, seqs), 1) == (iota((n_rows, seqs), 0) >> 2)
-    spread_f = spread.astype(F32)
-    spread_b = spread_f.astype(BF16)
-    q_rows = dot(perm, q_cat)
-    k_rows = dot(spread_b, key_new)
-    v_rows = dot(spread_b, value_new)
-    self_score = jnp.sum(q_rows * k_rows, axis=1, keepdims=True)
-    gate_rows = dot(spread_f, forget, precision=HIGH)
-    gate_rows = jnp.sum(
-        jnp.where(iota((n_rows, 4), 1) == (iota((n_rows, 4), 0) & 3), gate_rows, 0.0),
-        axis=1, keepdims=True)
+    by_head = (
+        jnp.where(low, q0, 0.0), jnp.where(low, pltpu.roll(q0, 64, 1), 0.0),
+        jnp.where(low, 0.0, pltpu.roll(q1, 64, 1)), jnp.where(low, 0.0, q1),
+    )
+    for h in range(4):
+        of_head = pl.ds(h, seqs, stride=4)
+        fanned[0, of_head, :] = by_head[h]
+        fanned[1, of_head, :] = key_new
+        fanned[2, of_head, :] = value_new
+        fanned[3, of_head, :] = jnp.broadcast_to(forget[:, h:h + 1], (seqs, 128))
+    q_rows = fanned[0]
+    v_rows = fanned[2]
+    self_score = jnp.sum(q_rows * fanned[1], axis=1, keepdims=True)
+    gate_rows = fanned[3][:, :1]
     q_rows = q_rows.astype(BF16)
 
-    phase("score")
-    phase("k_wait")
-    for p in range(pairs):
-        k_loads[p].wait()
-        v_loads[p].start()
-    phase("score2")
-    ready("lens", "gt")
     first = iota((8, 128), 0) < 4
     first_pos = iota((8, positions), 0) < 4
     pos = iota((8, positions), 1)
     for p in range(pairs):
+        if p == 0:
+            phase("k_wait0")
+            for copy in k_loads[:SPLIT // 2]:
+                copy.wait()
+            for copy in v_loads[SPLIT // 2:]:
+                copy.start()
+            load("wo", w_out, wo)
+            phase("score0")
+        if p == pairs // 2:
+            phase("k_wait1")
+            for copy in k_loads[SPLIT // 2:]:
+                copy.wait()
+            phase("score1")
         q8 = q_rows[8 * p:8 * p + 8, :]
         zero = jnp.zeros_like(q8)
         q_pair = jnp.concatenate(
@@ -267,28 +283,30 @@
     total = jnp.sum(weight, axis=1, keepdims=True) + self_weight
     scores[...] = weight / total
     self_prob = (self_weight / total).astype(BF16).astype(F32)
-    phase("values")
-    for item in later:
-        load(*item)
-    phase("v_wait")
     for p in range(pairs):
-        v_loads[p].wait()
-    phase("values2")
-    for p in range(pairs):
+        if p == 0:
+            phase("v_wait0")
+            for copy in v_loads[:SPLIT // 2]:
+                copy.wait()
+            for item in later:
+                load(*item)
+            phase("values0")
+        if p == pairs // 2:
+            phase("v_wait1")
+            for copy in v_loads[SPLIT // 2:]:
+                copy.wait()
+            ready("wo")
+            phase("values1")
         prob = scores[8 * p:8 * p + 8, :].astype(BF16)
         v_pair = jnp.concatenate([vc[2 * p], vc[2 * p + 1]], axis=1)
         mixed = dot(prob, v_pair)
         heads[8 * p:8 * p + 8, :] = jnp.where(first, mixed[:, :128], mixed[:, 128:])
-    mixed = heads[...] + self_prob * v_rows
-    row_high = (iota((n_rows, 128), 0) & 2) > 0
-    lane_high = iota((n_rows, 128), 1) >= 64
-    mixed = jnp.where(row_high == lane_high, mixed, 0.0).astype(BF16)
-    a_cat = dot(perm, mixed, TN)
-    a0, a1 = a_cat[:seqs], a_cat[seqs:2 * seqs]
-    a2, a3 = a_cat[2 * seqs:3 * seqs], a_cat[3 * seqs:]
-    attn = jnp.concatenate(
-        [a0 + pltpu.roll(a1, 64, 1), pltpu.roll(a2, 64, 1) + a3], axis=1).astype(BF16)
-    ready("wo")
+    heads[...] = heads[...] + self_prob * v_rows
+    a0, a1, a2, a3 = (
+        heads[pl.ds(h, seqs, stride=4), :].astype(BF16).astype(F32) for h in range(4))
+    attn = jnp.concatenate([
+        jnp.where(low, a0, pltpu.roll(a1, 64, 1)), jnp.where(low, pltpu.roll(a2, 64, 1), a3),
+    ], axis=1).astype(BF16)
     mine[...] = dot(attn, wo[...]).astype(BF16)
 
     phase("barrier")
@@ -305,18 +323,44 @@
     phase("norm2")
     residual = (
         tok[...].astype(F32) + (mine[...].astype(F32) + theirs[...].astype(F32))).astype(BF16)
+    kept[...] = residual
+    keep = pltpu.make_async_copy(kept, out_residual, fin_sem.at[2])
+    keep.start()
     ffn_rows = norm_rows(residual.astype(F32), gain2[...].reshape(1, width))
 
     phase("pack")
+
+    def lot(i):
+        return GROUPS if i == half - 1 else i // group
+
+    def landed(g, src, dst, send, recv, wait):
+        count = group - (g == GROUPS - 1)
+        if count:
+            part = pl.ds(g * group, count)
+            wait(pltpu.make_async_remote_copy(
+                src.at[part], dst.at[part], send.at[g], recv.at[g],
+                device_id=sibling, device_id_type=MESH))
+        if g == GROUPS - 1:
+            @pl.when(core == 1)
+            def _():
+                wait(pltpu.make_async_remote_copy(
+                    src.at[half - 1], dst.at[half - 1], send.at[GROUPS], recv.at[GROUPS],
+                    device_id=sibling, device_id_type=MESH))
+
+    def go_landed(g, wait):
+        landed(g, box_out, box_in, go_send, go_recv, wait)
+
+    def back_landed(g, wait):
+        landed(g, ret_out, ret_in, back_send, back_recv, wait)
 
     def go(i):
         return pltpu.make_async_remote_copy(
-            box_out.at[i], box_in.at[i], go_send.at[i], go_recv.at[i],
+            box_out.at[i], box_in.at[i], go_send.at[lot(i)], go_recv.at[lot(i)],
             device_id=(peer(i, True), core), device_id_type=MESH)
 
     def back(i):
         return pltpu.make_async_remote_copy(
-            ret_out.at[i], ret_in.at[i], back_send.at[i], back_recv.at[i],
+            ret_out.at[i], ret_in.at[i], back_send.at[lot(i)], back_recv.at[lot(i)],
             device_id=(peer(i, False), core), device_id_type=MESH)
 
     def members(g):
@@ -368,9 +412,12 @@
     total_rows[...] = dot(shared_h, sd[...])
 
     hidden_w = eg.shape[2]
+    phase("push_wait")
+    for push in pushes:
+        push.wait_recv()
     for g in range(GROUPS):
         phase(f"go_wait{g}")
-        each(members(g), lambda i: go(i).wait_recv())
+        go_landed(g, lambda copy: copy.wait_recv())
         phase(f"unpack{g}")
         lay[whole(g), :] = box_in[pl.ds(g * group, group)].reshape(
             g_rows * cols, 128).astype(F32)
@@ -378,9 +425,6 @@
             xs[:, 128 * j:128 * j + 128] = lay[lines(g, j), :].astype(BF16)
         phase(f"ffn_in{g}")
         for part in range(2):
-            if part == 1 and g == 0:
-                for push in pushes:
-                    push.wait_recv()
             gate = dot(xs[...], eg[part])
             up = dot(xs[...], eu[part])
             hid[:, hidden_w * part:hidden_w * (part + 1)] = (silu(gate) * up).astype(BF16)
@@ -401,7 +445,7 @@
 
     for g in range(GROUPS):
         phase(f"back_wait{g}")
-        each(members(g), lambda i: back(i).wait_recv())
+        back_landed(g, lambda copy: copy.wait_recv())
         phase(f"combine{g}")
         lay[whole(g), :] = ret_in[pl.ds(g * group, group)].reshape(
             g_rows * cols, 128).astype(F32)
@@ -417,18 +461,21 @@
 
     phase("finish")
     finish = pltpu.make_async_remote_copy(
-        fin_out, fin_in, fin_sem.at[0], fin_sem.at[1], device_id=sibling, device_id_type=MESH)
+        fin_out, out_theirs, fin_sem.at[0], fin_sem.at[1], device_id=sibling,
+        device_id_type=MESH)
     finish.start()
+    own = pltpu.make_async_copy(fin_out, out_mine, fin_sem.at[3])
+    own.start()
     swap.wait_send()
     for push in pushes:
         push.wait_send()
-    each(range(half), lambda i: go(i).wait_send())
-    each(range(half), lambda i: back(i).wait_send())
+    for g in range(GROUPS):
+        go_landed(g, lambda copy: copy.wait_send())
+        back_landed(g, lambda copy: copy.wait_send())
+    keep.wait()
+    own.wait()
+    finish.wait_send()
     finish.wait_recv()
-    phase("result")
-    out[...] = (
-        residual.astype(F32) + (fin_out[...].astype(F32) + fin_in[...].astype(F32))).astype(BF16)
-    finish.wait_send()
     phase()
 
 
@@ -466,23 +513,25 @@
         like(16),
         vmem((2, width, ff), BF16), vmem((2, width, ff), BF16), vmem((2, ff, width), BF16),
         vmem((4 * seqs, positions), F32), vmem((4 * seqs, 128), F32),
-        vmem((seqs, width), BF16), vmem((seqs, width), BF16),
+        vmem((4, 4 * seqs, 128), F32),
+        vmem((seqs, width), BF16), vmem((seqs, width), BF16), vmem((seqs, width), BF16),
         vmem((rows // GROUPS, width), BF16), vmem((rows // GROUPS, 2 * ff), BF16), vmem((rows * cols, 128), F32),
         vmem((half, CAP * cols, 128), BF16), vmem((half, CAP * cols, 128), BF16),
         vmem((half, CAP * cols, 128), BF16), vmem((half, CAP * cols, 128), BF16),
-        vmem((seqs, width), F32), vmem((seqs, width), BF16), vmem((seqs, width), BF16),
-        dma((18,)), dma((seqs // 2,)), dma((seqs // 2,)), dma((2,)), dma((3,)), dma((3,)),
-        dma((half,)), dma((half,)), dma((half,)), dma((half,)), dma((2,)),
+        vmem((seqs, width), F32), vmem((seqs, width), BF16),
+        dma((SLOTS,)), dma((SPLIT,)), dma((SPLIT,)), dma((2,)), dma((3,)), dma((3,)),
+        dma((GROUPS + 1,)), dma((GROUPS + 1,)), dma((GROUPS + 1,)), dma((GROUPS + 1,)), dma((4,)),
     ]
-    return pl.pallas_call(
+    residual, own, other = pl.pallas_call(
         functools.partial(kernel, split_dims(n_ep)),
-        out_shape=jax.ShapeDtypeStruct((seqs, width), BF16),
+        out_shape=[jax.ShapeDtypeStruct((seqs, width), BF16)] * 3,
         in_specs=[any_spec] * len(operands),
-        out_specs=pl.BlockSpec(memory_space=pltpu.VMEM),
+        out_specs=[any_spec] * 3,
         scratch_shapes=scratch,
         compiler_params=pltpu.CompilerParams(
             collective_id=0, has_side_effects=True, vmem_limit_bytes=62 * 1024 * 1024),
     )(*operands)
+    return (residual.astype(F32) + (own.astype(F32) + other.astype(F32))).astype(BF16)
 
 
 def solution(mesh):

time: 34.8 us -> 32.3 us (0.928)
  Pallas kernels: 33.1 us -> 30.6 us
  other arithmetic: 0 us -> 1.56 us
  local copies, waits for them, and re-layouts: 1.47 us -> 0 us
    pallas_call x1, Pallas kernels: 33.1 us -> 30.6 us  [per_device(): pl.pallas_call(functools.partial(kernel, split_dims(n_ep)), out_shape=[ja...]
    convert_element_type x0 -> x1, other arithmetic: none -> 1.56 us  [per_device(): (residual.astype(F32) + (own.astype(F32) + other.astype(F32))).astype(BF16)]
    unnamed x1 -> x0, local copies, waits for them, and re-layouts: 1.47 us -> none
where the time goes in v3:
time: 32.3 us; the launch traced here: 32.2 us
  Pallas kernels  30.6 us (95%)
  other arithmetic  1.56 us (5%)
    pallas_call x1, Pallas kernels, per_device(): pl.pallas_call(functools.partial(kernel, split_dims(n_ep)), out_shape=[ja...  30.6 us
    convert_element_type x1, other arithmetic, per_device(): (residual.astype(F32) + (own.astype(F32) + other.astype(F32))).astype(BF16)  1.56 us

profile of v3, /device:TPU:1, one launch (start us, length us, event | category | flops | bytes accessed | tf_op | source)
XLA Modules:
  0.0 32.2 jit_solution(7450657190517437255)
XLA Ops:
  0.0 30.6 %shard_map.190 = (bf16[16,2048]{1,0:T(8,128)(2,1)}, bf16[16,2048]{1,0:T(8,128)(2,1)}, bf16[16,2048]{1,0:T(8,128)(2,1)}) custom-call(bf16[16,2048]{1,0:T(8,128)(2,1)} %tokens.1, bf16[2048]{0:T(1024)(128)(2,1)} %norm_gain.1, bf16[2048,256]{1,0:T(8,128)(2,1)} %w_query.1, bf16[2048,128]{1,0:T(8,128)(2,1)} %w_key.1, bf16[2048,128]{1,0:T(8,128)(2,1)} %w_value.1, ...), custom_call_target="tpu_custom_call" | custom-call | tf_op jit(solution)/shard_map/pallas_call | solution.py:525
  30.6 1.6 %add_convert_fusion = bf16[16,2048]{1,0:T(8,128)(2,1)} fusion(bf16[16,2048]{1,0:T(8,128)(2,1)} %get-tuple-element.10, bf16[16,2048]{1,0:T(8,128)(2,1)} %get-tuple-element.9, bf16[16,2048]{1,0:T(8,128)(2,1)} %get-tuple-element.8), kind=kLoop, calls=%fused_computation | loop fusion | flops 196608 | bytes 262144 | tf_op jit(solution)/shard_map/convert_element_type | solution.py:534

commit v4 on v3

v4 whole, which is shorter than its diff:
```python
import functools

import jax
import jax.numpy as jnp
from jax import lax
from jax.experimental import pallas as pl
from jax.experimental.pallas import tpu as pltpu
from jax.sharding import PartitionSpec as P

HEAD_DIM = 64
EPS = 1e-06
ROUTE_SCALE = 2.5
CAP = 3
Z_STEP = 2
SLOTS = 9
SPLIT = 4
MESH = pl.DeviceIdType.MESH
F32 = jnp.float32
BF16 = jnp.bfloat16
HIGH = lax.Precision.HIGHEST
NT = (((1,), (1,)), ((), ()))
TN = (((0,), (0,)), ((), ()))
NN = (((1,), (0,)), ((), ()))


def dot(left, right, dims=NN, precision=None):
    return lax.dot_general(left, right, dims, precision=precision, preferred_element_type=F32)


def iota(shape, dim):
    return lax.broadcasted_iota(jnp.int32, shape, dim)


def norm_rows(values, gain):
    factor = lax.rsqrt(jnp.mean(values * values, axis=-1, keepdims=True) + EPS)
    return (values * factor * gain.astype(F32)).astype(BF16)


def silu(x):
    return x / (1.0 + jnp.exp(-x))


class Phases:
    def __init__(self):
        self.scope = None

    def __call__(self, name=None):
        if self.scope is not None:
            self.scope.__exit__(None, None, None)
        self.scope = jax.named_scope(name) if name else None
        if self.scope is not None:
            self.scope.__enter__()


def plane_tables(dims):
    ny, nx = dims[1:]

    def far(entry):
        return min(entry[0], ny - entry[0]) + min(entry[1], nx - entry[1])

    entries = [(dy, dx) for dy in range(ny) for dx in range(nx)]
    entries.sort(key=lambda entry: (-far(entry), entry))
    half = len(entries) // 2
    pairs, single = [], []
    for entry in entries:
        other = ((ny - entry[0]) % ny, (nx - entry[1]) % nx)
        if other == entry:
            single.append(entry)
        elif entry < other:
            pairs.append([entry, other])
    cut = len(pairs) // 2
    second = sum(pairs[:cut], [])
    fill = half - len(second)
    tables = (sum(pairs[cut:], []) + single[fill:], second + single[:fill])
    for table in tables:
        table.sort(key=lambda entry: -far(entry))
    assert len(tables[0]) == len(tables[1])
    return tables


def log2(n):
    assert n & (n - 1) == 0
    return n.bit_length() - 1


def kernel(
    dims,
    tokens, norm_gain, w_query, w_key, w_value, w_forget, w_out, cache_keys, cache_values,
    cache_gates, lengths, ffn_gain, router_w, routes, shared_gate, shared_up, shared_down,
    expert_gate, expert_up, expert_down,
    out_residual, out_mine, out_theirs,
    tok, gain1, wq, wk, wv, wf, wo, kc, vc, gt, lens, gain2, rw, rt, sg, su, sd,
    eg, eu, ed, scores, heads, fanned, mine, theirs, kept, xs, hid, lay, box_out, box_in, ret_out, ret_in,
    total_rows, fin_out,
    in_sem, k_sem, v_sem, att_sem, wt_send, wt_recv, go_send, go_recv, back_send, back_recv,
    fin_sem,
):
    nz, ny, nx = dims
    n_ep = nz * ny * nx
    half = n_ep // 2
    block = half // nz
    seqs, width = tokens.shape
    positions = cache_keys.shape[1]
    top_k = routes.shape[0]
    cols = width // 128
    rows = half * CAP
    b_rows = block * CAP
    z_step = min(Z_STEP, nz)
    pairs = seqs // 2
    ep = lax.axis_index("ep")
    core = lax.axis_index("tp")
    z, y, x = ep // (ny * nx), (ep // nx) % ny, ep % nx
    tables = plane_tables(dims)

    def by_core(first, second):
        return first if first == second else first + core * (second - first)

    def peer(dz, k, forward):
        dy, dx = (by_core(a, b) for a, b in zip(tables[0][k], tables[1][k]))
        if forward:
            pz, py, px = (z + dz) % nz, (y + dy) % ny, (x + dx) % nx
        else:
            pz, py, px = (z + nz - dz) % nz, (y + ny - dy) % ny, (x + nx - dx) % nx
        return (pz * ny + py) * nx + px

    def each(dz, action):
        for k in range(block - 1):
            action(k)
        here = jnp.logical_and(core == 0, dz == 0)
        pl.when(jnp.logical_not(here))(functools.partial(action, block - 1))

    phase = Phases()
    phase("loads")
    loads = {}
    order = (
        ("rt", routes, rt), ("tok", tokens, tok), ("gain1", norm_gain, gain1),
    )
    later = (
        ("rw", router_w, rw), ("gain2", ffn_gain, gain2),
        ("eg", expert_gate.at[0], eg.at[0]), ("eu", expert_up.at[0], eu.at[0]),
        ("ed", expert_down.at[0], ed.at[0]),
        ("sg", shared_gate, sg), ("su", shared_up, su), ("sd", shared_down, sd),
    )
    slot = 0

    def load(name, src, dst, pieces=1):
        nonlocal slot
        sem = in_sem.at[slot % SLOTS]
        loads[name] = pltpu.make_async_copy(src, dst, sem)
        size = src.shape[0] // pieces
        for n in range(pieces):
            part = pl.ds(n * size, size)
            if pieces == 1:
                loads[name].start()
            else:
                pltpu.make_async_copy(src.at[part], dst.at[part], sem).start()
        slot += 1

    def ready(*names):
        for name in names:
            loads[name].wait()

    for item in order:
        load(*item)
    load("wq", w_query, wq, 4)
    load("lens", lengths, lens)
    load("gt", cache_gates, gt)
    step = seqs // SPLIT

    def cache_copy(src, dst, sem, n):
        return pltpu.make_async_copy(
            src.at[pl.ds(n * step, step)], dst.at[pl.ds(n * step, step)], sem.at[n])

    k_loads = [cache_copy(cache_keys, kc, k_sem, n) for n in range(SPLIT)]
    v_loads = [cache_copy(cache_values, vc, v_sem, n) for n in range(SPLIT)]
    for copy in k_loads[:SPLIT // 2]:
        copy.start()

    phase("greet")
    barrier = pltpu.get_barrier_semaphore()

    for dz in range(nz):
        each(dz, lambda k: pl.semaphore_signal(
            barrier, inc=1, device_id=(peer(dz, k, True), core), device_id_type=MESH))
    pl.semaphore_signal(barrier, inc=1, device_id=(ep, 1 - core), device_id_type=MESH)

    phase("slots")
    ready("rt")
    for copy in k_loads[SPLIT // 2:]:
        copy.start()
    slot_id = iota((rows, 1), 0)
    magic = -(-4096 // CAP)
    assert all((l * magic) >> 12 == l // CAP for l in range(rows))
    peer_i = (slot_id * magic) >> 12
    rank_of = slot_id - peer_i * CAP
    lny, lnx, lb = log2(ny), log2(nx), log2(block)
    in_plane = peer_i & (block - 1)
    code = jnp.zeros_like(slot_id)
    for k in range(block):
        first, second = ((table[k][0] << lnx) + table[k][1] for table in tables)
        code = jnp.where(in_plane == k, by_core(first, second), code)
    dz, dy, dx = peer_i >> lb, code >> lnx, code & (nx - 1)
    expert_of = (
        (((z + dz) & (nz - 1)) << (lny + lnx)) + (((y + dy) & (ny - 1)) << lnx)
        + ((x + dx) & (nx - 1)))
    routed_to = rt[...]
    marks = jnp.zeros((rows, seqs), F32)
    marks_all = jnp.zeros((n_ep, seqs), F32)
    all_experts = iota((n_ep, seqs), 0)
    for k in range(top_k):
        marks = marks + (routed_to[k:k + 1, :] == expert_of).astype(F32)
        marks_all = marks_all + (routed_to[k:k + 1, :] == all_experts).astype(F32)
    earlier = (iota((seqs, seqs), 0) < iota((seqs, seqs), 1)).astype(F32)
    rank = dot(marks.astype(BF16), earlier.astype(BF16))
    pick = jnp.where(rank == rank_of.astype(F32), marks, 0.0)
    to_slot = (iota((rows, n_ep), 1) == expert_of).astype(F32)

    phase("project")
    ready("tok", "gain1", "wq")
    load("wk", w_key, wk)
    load("wv", w_value, wv)
    load("wf", w_forget, wf)
    for copy in v_loads[:SPLIT // 2]:
        copy.start()
    normed = norm_rows(tok[...].astype(F32), gain1[...].reshape(1, width))
    query = (dot(normed, wq[...]).astype(BF16).astype(F32)) * (HEAD_DIM ** -0.5)

    n_rows = 4 * seqs
    low = iota((seqs, 128), 1) < 64
    q0, q1 = query[:, :128], query[:, 128:]
    by_head = (
        jnp.where(low, q0, 0.0), jnp.where(low, pltpu.roll(q0, 64, 1), 0.0),
        jnp.where(low, 0.0, pltpu.roll(q1, 64, 1)), jnp.where(low, 0.0, q1),
    )
    for h in range(4):
        fanned[0, pl.ds(h, seqs, stride=4), :] = by_head[h]
    q_rows = fanned[0].astype(BF16)

    first = iota((8, 128), 0) < 4
    first_pos = iota((8, positions), 0) < 4
    pos = iota((8, positions), 1)
    for p in range(pairs):
        if p == 0:
            phase("k_wait0")
            ready("lens", "gt")
            for copy in k_loads[:SPLIT // 2]:
                copy.wait()
            for copy in v_loads[SPLIT // 2:]:
                copy.start()
            load("wo", w_out, wo)
            phase("score0")
        if p == pairs // 2:
            phase("k_wait1")
            for copy in k_loads[SPLIT // 2:]:
                copy.wait()
            phase("score1")
        q8 = q_rows[8 * p:8 * p + 8, :]
        zero = jnp.zeros_like(q8)
        q_pair = jnp.concatenate(
            [jnp.where(first, q8, zero), jnp.where(first, zero, q8)], axis=1)
        k_pair = jnp.concatenate([kc[2 * p], kc[2 * p + 1]], axis=1)
        s = dot(q_pair, k_pair, NT)
        g = jnp.concatenate([gt[2 * p], gt[2 * p + 1]], axis=0)
        count = jnp.where(first_pos, lens[2 * p], lens[2 * p + 1])
        last = jnp.sum(jnp.where(pos == count - 1, g, 0.0), axis=1, keepdims=True)
        s = s + (last - g)
        scores[8 * p:8 * p + 8, :] = jnp.where(pos < count, s, -jnp.inf)
    phase("project_kv")
    ready("wk", "wv", "wf")
    key_new = dot(normed, wk[...]).astype(BF16).astype(F32)
    value_new = dot(normed, wv[...]).astype(BF16).astype(F32)
    forget = dot(normed, wf[...], NT)
    forget = jnp.minimum(forget, 0.0) - jnp.log1p(jnp.exp(-jnp.abs(forget)))
    for h in range(4):
        of_head = pl.ds(h, seqs, stride=4)
        fanned[1, of_head, :] = key_new
        fanned[2, of_head, :] = value_new
        fanned[3, of_head, :] = jnp.broadcast_to(forget[:, h:h + 1], (seqs, 128))
    phase("softmax")
    self_score = jnp.sum(fanned[0] * fanned[1], axis=1, keepdims=True)
    s = scores[...] + fanned[3][:, :1]
    peak = jnp.maximum(jnp.max(s, axis=1, keepdims=True), self_score)
    weight = jnp.exp(s - peak)
    self_weight = jnp.exp(self_score - peak)
    total = jnp.sum(weight, axis=1, keepdims=True) + self_weight
    scores[...] = weight / total
    self_prob = (self_weight / total).astype(BF16).astype(F32)
    for p in range(pairs):
        if p == 0:
            phase("v_wait0")
            for copy in v_loads[:SPLIT // 2]:
                copy.wait()
            for item in later:
                load(*item)
            phase("values0")
        if p == pairs // 2:
            phase("v_wait1")
            for copy in v_loads[SPLIT // 2:]:
                copy.wait()
            ready("wo")
            phase("values1")
        prob = scores[8 * p:8 * p + 8, :].astype(BF16)
        v_pair = jnp.concatenate([vc[2 * p], vc[2 * p + 1]], axis=1)
        mixed = dot(prob, v_pair)
        heads[8 * p:8 * p + 8, :] = jnp.where(first, mixed[:, :128], mixed[:, 128:])
    heads[...] = heads[...] + self_prob * fanned[2]
    a0, a1, a2, a3 = (
        heads[pl.ds(h, seqs, stride=4), :].astype(BF16).astype(F32) for h in range(4))
    attn = jnp.concatenate([
        jnp.where(low, a0, pltpu.roll(a1, 64, 1)), jnp.where(low, pltpu.roll(a2, 64, 1), a3),
    ], axis=1).astype(BF16)
    mine[...] = dot(attn, wo[...]).astype(BF16)

    phase("barrier")
    pl.semaphore_wait(barrier, half + core)

    phase("swap_start")
    sibling = (ep, 1 - core)
    swap = pltpu.make_async_remote_copy(
        mine, theirs, att_sem.at[0], att_sem.at[1], device_id=sibling, device_id_type=MESH)
    swap.start()
    ready("gain2")
    phase("swap_wait")
    swap.wait_recv()
    phase("norm2")
    residual = (
        tok[...].astype(F32) + (mine[...].astype(F32) + theirs[...].astype(F32))).astype(BF16)
    kept[...] = residual
    keep = pltpu.make_async_copy(kept, out_residual, fin_sem.at[2])
    keep.start()
    ffn_rows = norm_rows(residual.astype(F32), gain2[...].reshape(1, width))

    phase("pack")

    def landed(dz, src, dst, send, recv, wait):
        def take(count):
            part = pl.ds(dz * block, count)
            wait(pltpu.make_async_remote_copy(
                src.at[part], dst.at[part], send.at[dz], recv.at[dz],
                device_id=sibling, device_id_type=MESH))

        here = jnp.logical_and(core == 0, dz == 0)
        pl.when(here)(lambda: take(block - 1) if block > 1 else None)
        pl.when(jnp.logical_not(here))(lambda: take(block))

    def go_landed(dz, wait):
        landed(dz, box_out, box_in, go_send, go_recv, wait)

    def back_landed(dz, wait):
        landed(dz, ret_out, ret_in, back_send, back_recv, wait)

    def go(dz, k):
        i = dz * block + k
        return pltpu.make_async_remote_copy(
            box_out.at[i], box_in.at[i], go_send.at[dz], go_recv.at[dz],
            device_id=(peer(dz, k, True), core), device_id_type=MESH)

    def back(dz, k):
        i = dz * block + k
        return pltpu.make_async_remote_copy(
            ret_out.at[i], ret_in.at[i], back_send.at[dz], back_recv.at[dz],
            device_id=(peer(dz, k, False), core), device_id_type=MESH)

    far_z = sorted(range(nz), key=lambda dz: -min(dz, nz - dz))
    lines = [pl.ds(j, b_rows, stride=cols) for j in range(cols)]
    box_shape = (block, CAP * cols, 128)

    for dz in far_z:
        chosen = pick[dz * b_rows:(dz + 1) * b_rows].astype(BF16)
        stage = lay.at[dz % z_step]
        for j in range(cols // 2):
            part = dot(chosen, ffn_rows[:, 256 * j:256 * j + 256])
            stage[lines[2 * j], :] = part[:, :128]
            stage[lines[2 * j + 1], :] = part[:, 128:]
        box_out[pl.ds(dz * block, block)] = stage[...].astype(BF16).reshape(box_shape)
        each(dz, lambda k: go(dz, k).start())

    @pl.when(core == 0)
    def _():
        box_in[block - 1] = box_out[block - 1]

    ready("eg", "eu", "ed")
    pushes = [
        pltpu.make_async_remote_copy(
            buf.at[0], buf.at[1], wt_send.at[n], wt_recv.at[n], device_id=sibling,
            device_id_type=MESH)
        for n, buf in enumerate((eg, eu, ed))
    ]
    for push in pushes:
        push.start()

    phase("shared")
    ready("rw")
    chance = dot(rw[...], ffn_rows, NT)
    chance = marks_all / (1.0 + jnp.exp(-chance))
    share = ROUTE_SCALE * chance / jnp.sum(chance, axis=0, keepdims=True)
    slot_w = dot(to_slot, share, precision=HIGH) * pick
    slot_hi = slot_w.astype(BF16).astype(F32)
    slot_w = jnp.concatenate([slot_hi, slot_w - slot_hi], axis=1)
    mix = [
        jnp.transpose(slot_w[dz * b_rows:(dz + 1) * b_rows]).astype(BF16) for dz in range(nz)
    ]
    ready("sg", "su", "sd")
    shared_h = (silu(dot(ffn_rows, sg[...])) * dot(ffn_rows, su[...])).astype(BF16)
    total_rows[...] = dot(shared_h, sd[...])

    hidden_w = eg.shape[2]
    phase("push_wait")
    for push in pushes:
        push.wait_recv()
    for first_z in range(0, nz, z_step):
        from_z = [(z + nz - first_z - n) % nz for n in range(z_step)]
        phase(f"go_wait{first_z}")
        for dz in from_z:
            go_landed(dz, lambda copy: copy.wait_recv())
        phase(f"unpack{first_z}")
        for n, dz in enumerate(from_z):
            lay[n] = box_in[pl.ds(dz * block, block)].reshape(b_rows * cols, 128).astype(F32)
        for j in range(cols):
            xs[:, 128 * j:128 * j + 128] = jnp.concatenate(
                [lay.at[n][lines[j], :] for n in range(z_step)], axis=0).astype(BF16)
        phase(f"ffn_in{first_z}")
        for part in range(2):
            gate = dot(xs[...], eg[part])
            up = dot(xs[...], eu[part])
            hid[:, hidden_w * part:hidden_w * (part + 1)] = (silu(gate) * up).astype(BF16)
        phase(f"ffn_out{first_z}")
        for j in range(cols // 2):
            down = ed[:, :, 256 * j:256 * j + 256].reshape(2 * hidden_w, 256)
            answer = dot(hid[...], down)
            for n in range(z_step):
                piece = answer[n * b_rows:(n + 1) * b_rows]
                lay.at[n][lines[2 * j], :] = piece[:, :128]
                lay.at[n][lines[2 * j + 1], :] = piece[:, 128:]
        for n, dz in enumerate(from_z):
            ret_out[pl.ds(dz * block, block)] = lay[n].astype(BF16).reshape(box_shape)
        phase(f"back_start{first_z}")
        for dz in from_z:
            each(dz, lambda k: back(dz, k).start())

    @pl.when(core == 0)
    def _():
        ret_in[block - 1] = ret_out[block - 1]

    near_z = far_z[::-1]
    for m in range(0, nz, z_step):
        phase(f"back_wait{m}")
        some = near_z[m:m + z_step]
        for dz in some:
            back_landed(dz, lambda copy: copy.wait_recv())
        phase(f"combine{m}")
        for n, dz in enumerate(some):
            lay[n] = ret_in[pl.ds(dz * block, block)].reshape(b_rows * cols, 128).astype(F32)
        for j in range(cols // 2):
            span = slice(256 * j, 256 * j + 256)
            part = total_rows[:, span]
            for n, dz in enumerate(some):
                answer = jnp.concatenate(
                    [lay.at[n][lines[2 * j], :], lay.at[n][lines[2 * j + 1], :]],
                    axis=1).astype(BF16)
                both = dot(mix[dz], answer)
                part = part + (both[:seqs] + both[seqs:])
            if m + z_step < nz:
                total_rows[:, span] = part
            else:
                fin_out[:, span] = part.astype(BF16)

    phase("finish")
    finish = pltpu.make_async_remote_copy(
        fin_out, out_theirs, fin_sem.at[0], fin_sem.at[1], device_id=sibling,
        device_id_type=MESH)
    finish.start()
    own = pltpu.make_async_copy(fin_out, out_mine, fin_sem.at[3])
    own.start()
    swap.wait_send()
    for push in pushes:
        push.wait_send()
    for dz in range(nz):
        go_landed(dz, lambda copy: copy.wait_send())
        back_landed(dz, lambda copy: copy.wait_send())
    keep.wait()
    own.wait()
    finish.wait_send()
    finish.wait_recv()
    phase()


def split_dims(n):
    return {64: (4, 4, 4), 4: (1, 2, 2), 8: (2, 2, 2)}[n]


def per_device(
    tokens, norm_gain, w_query, w_key, w_value, w_forget, w_out, cache_keys, cache_values,
    cache_gates, lengths, ffn_gain, router_w, routes, shared_gate, shared_up, shared_down,
    expert_gate, expert_up, expert_down,
):
    seqs, width = tokens.shape
    n_ep = lax.axis_size("ep")
    half = n_ep // 2
    dims = split_dims(n_ep)
    z_step = min(Z_STEP, dims[0])
    step_rows = half * CAP // dims[0] * z_step
    cols = width // 128
    positions = cache_keys.shape[1]
    ff = expert_gate.shape[2]
    any_spec = pl.BlockSpec(memory_space=pl.ANY)
    operands = (
        tokens, norm_gain, w_query, w_key, w_value, w_forget.T, w_out,
        cache_keys, cache_values, cache_gates, lengths, ffn_gain, router_w.T,
        routes.T, shared_gate, shared_up, shared_down, expert_gate, expert_up, expert_down,
    )
    vmem = pltpu.VMEM
    dma = pltpu.SemaphoreType.DMA

    def like(index):
        return vmem(operands[index].shape, operands[index].dtype)

    scratch = [
        like(0), like(1), like(2), like(3), like(4), like(5), like(6), like(7), like(8), like(9),
        pltpu.SMEM(lengths.shape, jnp.int32), like(11), like(12), like(13), like(14), like(15),
        like(16),
        vmem((2, width, ff), BF16), vmem((2, width, ff), BF16), vmem((2, ff, width), BF16),
        vmem((4 * seqs, positions), F32), vmem((4 * seqs, 128), F32),
        vmem((4, 4 * seqs, 128), F32),
        vmem((seqs, width), BF16), vmem((seqs, width), BF16), vmem((seqs, width), BF16),
        vmem((step_rows, width), BF16), vmem((step_rows, 2 * ff), BF16),
        vmem((z_step, step_rows // z_step * cols, 128), F32),
        vmem((half, CAP * cols, 128), BF16), vmem((half, CAP * cols, 128), BF16),
        vmem((half, CAP * cols, 128), BF16), vmem((half, CAP * cols, 128), BF16),
        vmem((seqs, width), F32), vmem((seqs, width), BF16),
        dma((SLOTS,)), dma((SPLIT,)), dma((SPLIT,)), dma((2,)), dma((3,)), dma((3,)),
        dma((dims[0],)), dma((dims[0],)), dma((dims[0],)), dma((dims[0],)), dma((4,)),
    ]
    residual, own, other = pl.pallas_call(
        functools.partial(kernel, dims),
        out_shape=[jax.ShapeDtypeStruct((seqs, width), BF16)] * 3,
        in_specs=[any_spec] * len(operands),
        out_specs=[any_spec] * 3,
        scratch_shapes=scratch,
        compiler_params=pltpu.CompilerParams(
            collective_id=0, has_side_effects=True, vmem_limit_bytes=62 * 1024 * 1024),
    )(*operands)
    return (residual.astype(F32) + (own.astype(F32) + other.astype(F32))).astype(BF16)


def solution(mesh):
    placed = (
        P("ep", None),
        P(),
        P(None, "tp"),
        P(None, "tp"),
        P(None, "tp"),
        P(None, "tp"),
        P("tp", None),
        P("ep", None, "tp"),
        P("ep", None, "tp"),
        P("ep", "tp", None),
        P("ep"),
        P(),
        P(),
        P("ep", None),
        P(None, "tp"),
        P(None, "tp"),
        P("tp", None),
        P("ep", None, "tp"),
        P("ep", None, "tp"),
        P("ep", "tp", None),
    )
    return jax.shard_map(
        per_device, mesh=mesh, in_specs=placed, out_specs=P("ep", None), check_vma=False
    )
```

time: 32.3 us -> 29.8 us (0.923)
  Pallas kernels: 30.6 us -> 28.1 us
    pallas_call x1, Pallas kernels: 30.6 us -> 28.1 us  [per_device(): pl.pallas_call(functools.partial(kernel, dims), out_shape=[jax.ShapeDtype...]
where the time goes in v4:
time: 29.8 us; the launch traced here: 29.7 us
  Pallas kernels  28.1 us (94%)
  other arithmetic  1.56 us (5%)
    pallas_call x1, Pallas kernels, per_device(): pl.pallas_call(functools.partial(kernel, dims), out_shape=[jax.ShapeDtype...  28.1 us
    convert_element_type x1, other arithmetic, per_device(): (residual.astype(F32) + (own.astype(F32) + other.astype(F32))).astype(BF16)  1.56 us

profile of v4, /device:TPU:1, one launch (start us, length us, event | category | flops | bytes accessed | tf_op | source)
XLA Modules:
  0.0 29.7 jit_solution(9406261903738859648)
XLA Ops:
  0.0 28.1 %shard_map.190 = (bf16[16,2048]{1,0:T(8,128)(2,1)}, bf16[16,2048]{1,0:T(8,128)(2,1)}, bf16[16,2048]{1,0:T(8,128)(2,1)}) custom-call(bf16[16,2048]{1,0:T(8,128)(2,1)} %tokens.1, bf16[2048]{0:T(1024)(128)(2,1)} %norm_gain.1, bf16[2048,256]{1,0:T(8,128)(2,1)} %w_query.1, bf16[2048,128]{1,0:T(8,128)(2,1)} %w_key.1, bf16[2048,128]{1,0:T(8,128)(2,1)} %w_value.1, ...), custom_call_target="tpu_custom_call" | custom-call | tf_op jit(solution)/shard_map/pallas_call | solution.py:534
  28.1 1.6 %add_convert_fusion = bf16[16,2048]{1,0:T(8,128)(2,1)} fusion(bf16[16,2048]{1,0:T(8,128)(2,1)} %get-tuple-element.10, bf16[16,2048]{1,0:T(8,128)(2,1)} %get-tuple-element.9, bf16[16,2048]{1,0:T(8,128)(2,1)} %get-tuple-element.8), kind=kLoop, calls=%fused_computation | loop fusion | flops 196608 | bytes 262144 | tf_op jit(solution)/shard_map/convert_element_type | solution.py:543

commit v5 on v4

--- a/solution.py
+++ b/solution.py
@@ -13,7 +13,7 @@
 CAP = 3
 Z_STEP = 2
 SLOTS = 9
-SPLIT = 4
+PIECES = 2
 MESH = pl.DeviceIdType.MESH
 F32 = jnp.float32
 BF16 = jnp.bfloat16
@@ -90,8 +90,8 @@
     expert_gate, expert_up, expert_down,
     out_residual, out_mine, out_theirs,
     tok, gain1, wq, wk, wv, wf, wo, kc, vc, gt, lens, gain2, rw, rt, sg, su, sd,
-    eg, eu, ed, scores, heads, fanned, mine, theirs, kept, xs, hid, lay, box_out, box_in, ret_out, ret_in,
-    total_rows, fin_out,
+    eg, eu, ed, scores, heads, fanned, mine, theirs, xs, hid, lay, box_out, box_in, ret_out, ret_in,
+    total_rows,
     in_sem, k_sem, v_sem, att_sem, wt_send, wt_recv, go_send, go_recv, back_send, back_recv,
     fin_sem,
 ):
@@ -165,29 +165,30 @@
     load("wq", w_query, wq, 4)
     load("lens", lengths, lens)
     load("gt", cache_gates, gt)
-    step = seqs // SPLIT
-
-    def cache_copy(src, dst, sem, n):
-        return pltpu.make_async_copy(
-            src.at[pl.ds(n * step, step)], dst.at[pl.ds(n * step, step)], sem.at[n])
-
-    k_loads = [cache_copy(cache_keys, kc, k_sem, n) for n in range(SPLIT)]
-    v_loads = [cache_copy(cache_values, vc, v_sem, n) for n in range(SPLIT)]
-    for copy in k_loads[:SPLIT // 2]:
-        copy.start()
+    step = seqs // (2 * PIECES)
+
+    def cache_half(src, dst, sem, n):
+        for piece in range(PIECES):
+            part = pl.ds((n * PIECES + piece) * step, step)
+            pltpu.make_async_copy(src.at[part], dst.at[part], sem.at[n]).start()
+        part = pl.ds(n * PIECES * step, PIECES * step)
+        return pltpu.make_async_copy(src.at[part], dst.at[part], sem.at[n])
+
+    k_half = [cache_half(cache_keys, kc, k_sem, 0)]
+    v_half = []
 
     phase("greet")
     barrier = pltpu.get_barrier_semaphore()
 
-    for dz in range(nz):
+    far_z = sorted(range(nz), key=lambda dz: -min(dz, nz - dz))
+    for dz in far_z:
         each(dz, lambda k: pl.semaphore_signal(
             barrier, inc=1, device_id=(peer(dz, k, True), core), device_id_type=MESH))
     pl.semaphore_signal(barrier, inc=1, device_id=(ep, 1 - core), device_id_type=MESH)
 
     phase("slots")
     ready("rt")
-    for copy in k_loads[SPLIT // 2:]:
-        copy.start()
+    k_half.append(cache_half(cache_keys, kc, k_sem, 1))
     slot_id = iota((rows, 1), 0)
     magic = -(-4096 // CAP)
     assert all((l * magic) >> 12 == l // CAP for l in range(rows))
@@ -220,8 +221,7 @@
     load("wk", w_key, wk)
     load("wv", w_value, wv)
     load("wf", w_forget, wf)
-    for copy in v_loads[:SPLIT // 2]:
-        copy.start()
+    v_half.append(cache_half(cache_values, vc, v_sem, 0))
     normed = norm_rows(tok[...].astype(F32), gain1[...].reshape(1, width))
     query = (dot(normed, wq[...]).astype(BF16).astype(F32)) * (HEAD_DIM ** -0.5)
 
@@ -243,16 +243,13 @@
         if p == 0:
             phase("k_wait0")
             ready("lens", "gt")
-            for copy in k_loads[:SPLIT // 2]:
-                copy.wait()
-            for copy in v_loads[SPLIT // 2:]:
-                copy.start()
+            k_half[0].wait()
+            v_half.append(cache_half(cache_values, vc, v_sem, 1))
             load("wo", w_out, wo)
             phase("score0")
         if p == pairs // 2:
             phase("k_wait1")
-            for copy in k_loads[SPLIT // 2:]:
-                copy.wait()
+            k_half[1].wait()
             phase("score1")
         q8 = q_rows[8 * p:8 * p + 8, :]
         zero = jnp.zeros_like(q8)
@@ -288,15 +285,13 @@
     for p in range(pairs):
         if p == 0:
             phase("v_wait0")
-            for copy in v_loads[:SPLIT // 2]:
-                copy.wait()
+            v_half[0].wait()
             for item in later:
                 load(*item)
             phase("values0")
         if p == pairs // 2:
             phase("v_wait1")
-            for copy in v_loads[SPLIT // 2:]:
-                copy.wait()
+            v_half[1].wait()
             ready("wo")
             phase("values1")
         prob = scores[8 * p:8 * p + 8, :].astype(BF16)
@@ -325,43 +320,50 @@
     phase("norm2")
     residual = (
         tok[...].astype(F32) + (mine[...].astype(F32) + theirs[...].astype(F32))).astype(BF16)
-    kept[...] = residual
-    keep = pltpu.make_async_copy(kept, out_residual, fin_sem.at[2])
-    keep.start()
+    out_residual[...] = residual
     ffn_rows = norm_rows(residual.astype(F32), gain2[...].reshape(1, width))
 
     phase("pack")
 
-    def landed(dz, src, dst, send, recv, wait):
+    def landed(dz, src, dst, send, recv):
         def take(count):
             part = pl.ds(dz * block, count)
-            wait(pltpu.make_async_remote_copy(
-                src.at[part], dst.at[part], send.at[dz], recv.at[dz],
-                device_id=sibling, device_id_type=MESH))
+            pltpu.make_async_remote_copy(
+                src.at[part], dst.at[part], send.at[0], recv.at[dz],
+                device_id=sibling, device_id_type=MESH).wait_recv()
 
         here = jnp.logical_and(core == 0, dz == 0)
         pl.when(here)(lambda: take(block - 1) if block > 1 else None)
         pl.when(jnp.logical_not(here))(lambda: take(block))
 
-    def go_landed(dz, wait):
-        landed(dz, box_out, box_in, go_send, go_recv, wait)
-
-    def back_landed(dz, wait):
-        landed(dz, ret_out, ret_in, back_send, back_recv, wait)
+    def go_landed(dz):
+        landed(dz, box_out, box_in, go_send, go_recv)
+
+    def back_landed(dz):
+        landed(dz, ret_out, ret_in, back_send, back_recv)
+
+    def sent(src, dst, send, recv):
+        def take(count):
+            part = pl.ds(0, count)
+            pltpu.make_async_remote_copy(
+                src.at[part], dst.at[part], send.at[0], recv.at[0],
+                device_id=sibling, device_id_type=MESH).wait_send()
+
+        pl.when(core == 0)(lambda: take(half - 1))
+        pl.when(core == 1)(lambda: take(half))
 
     def go(dz, k):
         i = dz * block + k
         return pltpu.make_async_remote_copy(
-            box_out.at[i], box_in.at[i], go_send.at[dz], go_recv.at[dz],
+            box_out.at[i], box_in.at[i], go_send.at[0], go_recv.at[dz],
             device_id=(peer(dz, k, True), core), device_id_type=MESH)
 
     def back(dz, k):
         i = dz * block + k
         return pltpu.make_async_remote_copy(
-            ret_out.at[i], ret_in.at[i], back_send.at[dz], back_recv.at[dz],
+            ret_out.at[i], ret_in.at[i], back_send.at[0], back_recv.at[dz],
             device_id=(peer(dz, k, False), core), device_id_type=MESH)
 
-    far_z = sorted(range(nz), key=lambda dz: -min(dz, nz - dz))
     lines = [pl.ds(j, b_rows, stride=cols) for j in range(cols)]
     box_shape = (block, CAP * cols, 128)
 
@@ -412,7 +414,7 @@
         from_z = [(z + nz - first_z - n) % nz for n in range(z_step)]
         phase(f"go_wait{first_z}")
         for dz in from_z:
-            go_landed(dz, lambda copy: copy.wait_recv())
+            go_landed(dz)
         phase(f"unpack{first_z}")
         for n, dz in enumerate(from_z):
             lay[n] = box_in[pl.ds(dz * block, block)].reshape(b_rows * cols, 128).astype(F32)
@@ -443,11 +445,11 @@
         ret_in[block - 1] = ret_out[block - 1]
 
     near_z = far_z[::-1]
-    for m in range(0, nz, z_step):
+    lots = [near_z[:z_step]] + [[dz] for dz in near_z[z_step:]]
+    for m, some in enumerate(lots):
         phase(f"back_wait{m}")
-        some = near_z[m:m + z_step]
         for dz in some:
-            back_landed(dz, lambda copy: copy.wait_recv())
+            back_landed(dz)
         phase(f"combine{m}")
         for n, dz in enumerate(some):
             lay[n] = ret_in[pl.ds(dz * block, block)].reshape(b_rows * cols, 128).astype(F32)
@@ -460,26 +462,21 @@
                     axis=1).astype(BF16)
                 both = dot(mix[dz], answer)
                 part = part + (both[:seqs] + both[seqs:])
-            if m + z_step < nz:
+            if m + 1 < len(lots):
                 total_rows[:, span] = part
             else:
-                fin_out[:, span] = part.astype(BF16)
+                out_mine[:, span] = part.astype(BF16)
 
     phase("finish")
     finish = pltpu.make_async_remote_copy(
-        fin_out, out_theirs, fin_sem.at[0], fin_sem.at[1], device_id=sibling,
+        out_mine, out_theirs, fin_sem.at[0], fin_sem.at[1], device_id=sibling,
         device_id_type=MESH)
     finish.start()
-    own = pltpu.make_async_copy(fin_out, out_mine, fin_sem.at[3])
-    own.start()
     swap.wait_send()
     for push in pushes:
         push.wait_send()
-    for dz in range(nz):
-        go_landed(dz, lambda copy: copy.wait_send())
-        back_landed(dz, lambda copy: copy.wait_send())
-    keep.wait()
-    own.wait()
+    sent(box_out, box_in, go_send, go_recv)
+    sent(ret_out, ret_in, back_send, back_recv)
     finish.wait_send()
     finish.wait_recv()
     phase()
@@ -509,6 +506,8 @@
         cache_keys, cache_values, cache_gates, lengths, ffn_gain, router_w.T,
         routes.T, shared_gate, shared_up, shared_down, expert_gate, expert_up, expert_down,
     )
+    operands = tuple(
+        pltpu.with_memory_space_constraint(operand, pltpu.HBM) for operand in operands)
     vmem = pltpu.VMEM
     dma = pltpu.SemaphoreType.DMA
 
@@ -522,23 +521,23 @@
         vmem((2, width, ff), BF16), vmem((2, width, ff), BF16), vmem((2, ff, width), BF16),
         vmem((4 * seqs, positions), F32), vmem((4 * seqs, 128), F32),
         vmem((4, 4 * seqs, 128), F32),
-        vmem((seqs, width), BF16), vmem((seqs, width), BF16), vmem((seqs, width), BF16),
+        vmem((seqs, width), BF16), vmem((seqs, width), BF16),
         vmem((step_rows, width), BF16), vmem((step_rows, 2 * ff), BF16),
         vmem((z_step, step_rows // z_step * cols, 128), F32),
         vmem((half, CAP * cols, 128), BF16), vmem((half, CAP * cols, 128), BF16),
         vmem((half, CAP * cols, 128), BF16), vmem((half, CAP * cols, 128), BF16),
-        vmem((seqs, width), F32), vmem((seqs, width), BF16),
-        dma((SLOTS,)), dma((SPLIT,)), dma((SPLIT,)), dma((2,)), dma((3,)), dma((3,)),
-        dma((dims[0],)), dma((dims[0],)), dma((dims[0],)), dma((dims[0],)), dma((4,)),
+        vmem((seqs, width), F32),
+        dma((SLOTS,)), dma((2,)), dma((2,)), dma((2,)), dma((3,)), dma((3,)),
+        dma((1,)), dma((dims[0],)), dma((1,)), dma((dims[0],)), dma((2,)),
     ]
     residual, own, other = pl.pallas_call(
         functools.partial(kernel, dims),
         out_shape=[jax.ShapeDtypeStruct((seqs, width), BF16)] * 3,
         in_specs=[any_spec] * len(operands),
-        out_specs=[any_spec] * 3,
+        out_specs=[pl.BlockSpec(memory_space=pltpu.VMEM)] * 3,
         scratch_shapes=scratch,
         compiler_params=pltpu.CompilerParams(
-            collective_id=0, has_side_effects=True, vmem_limit_bytes=62 * 1024 * 1024),
+            collective_id=0, has_side_effects=True, vmem_limit_bytes=32 * 1024 * 1024),
     )(*operands)
     return (residual.astype(F32) + (own.astype(F32) + other.astype(F32))).astype(BF16)
 

time: 29.8 us -> 28.7 us (0.963)
  other arithmetic: 1.56 us -> 0.66 us
    convert_element_type x1, other arithmetic: 1.56 us -> 0.66 us  [per_device(): (residual.astype(F32) + (own.astype(F32) + other.astype(F32))).astype(BF16)]
where the time goes in v5:
time: 28.7 us; the launch traced here: 28.6 us
  Pallas kernels  27.9 us (97%)
  other arithmetic  0.66 us (2%)
    pallas_call x1, Pallas kernels, per_device(): pl.pallas_call(functools.partial(kernel, dims), out_shape=[jax.ShapeDtype...  27.9 us
    convert_element_type x1, other arithmetic, per_device(): (residual.astype(F32) + (own.astype(F32) + other.astype(F32))).astype(BF16)  0.66 us

profile of v5, /device:TPU:1, one launch (start us, length us, event | category | flops | bytes accessed | tf_op | source)
XLA Modules:
  0.0 28.6 jit_solution(2094765884181719753)
XLA Ops:
  0.0 27.9 %shard_map.190 = (bf16[16,2048]{1,0:T(8,128)(2,1)S(1)}, bf16[16,2048]{1,0:T(8,128)(2,1)S(1)}, bf16[16,2048]{1,0:T(8,128)(2,1)S(1)}) custom-call(bf16[16,2048]{1,0:T(8,128)(2,1)} %tokens.1, bf16[2048]{0:T(1024)(128)(2,1)} %norm_gain.1, bf16[2048,256]{1,0:T(8,128)(2,1)} %w_query.1, bf16[2048,128]{1,0:T(8,128)(2,1)} %w_key.1, bf16[2048,128]{1,0:T(8,128)(2,1)} %w_value.1, ...), custom_call_target="tpu_custom_call" | custom-call | tf_op jit(solution)/shard_map/pallas_call | solution.py:533
  27.9 0.7 %add_convert_fusion = bf16[16,2048]{1,0:T(8,128)(2,1)} fusion(bf16[16,2048]{1,0:T(8,128)(2,1)S(1)} %get-tuple-element.10, bf16[16,2048]{1,0:T(8,128)(2,1)S(1)} %get-tuple-element.9, bf16[16,2048]{1,0:T(8,128)(2,1)S(1)} %get-tuple-element.8), kind=kLoop, calls=%fused_computation | loop fusion | flops 196608 | bytes 262144 | tf_op jit(solution)/shard_map/convert_element_type | solution.py:542

commit v6 on v5

--- a/solution.py
+++ b/solution.py
@@ -11,7 +11,7 @@
 EPS = 1e-06
 ROUTE_SCALE = 2.5
 CAP = 3
-Z_STEP = 2
+Z_STEP = 3
 SLOTS = 9
 PIECES = 2
 MESH = pl.DeviceIdType.MESH
@@ -367,7 +367,7 @@
     lines = [pl.ds(j, b_rows, stride=cols) for j in range(cols)]
     box_shape = (block, CAP * cols, 128)
 
-    for dz in far_z:
+    for dz in sorted(range(nz), key=lambda dz: (-min(dz, nz - dz), -dz)):
         chosen = pick[dz * b_rows:(dz + 1) * b_rows].astype(BF16)
         stage = lay.at[dz % z_step]
         for j in range(cols // 2):
@@ -410,8 +410,10 @@
     phase("push_wait")
     for push in pushes:
         push.wait_recv()
-    for first_z in range(0, nz, z_step):
-        from_z = [(z + nz - first_z - n) % nz for n in range(z_step)]
+    singles = nz - z_step
+    for some_z in [[n] for n in range(singles)] + [list(range(singles, nz))]:
+        first_z, count = some_z[0], len(some_z) * b_rows
+        from_z = [(z + nz - n) % nz for n in some_z]
         phase(f"go_wait{first_z}")
         for dz in from_z:
             go_landed(dz)
@@ -419,33 +421,31 @@
         for n, dz in enumerate(from_z):
             lay[n] = box_in[pl.ds(dz * block, block)].reshape(b_rows * cols, 128).astype(F32)
         for j in range(cols):
-            xs[:, 128 * j:128 * j + 128] = jnp.concatenate(
-                [lay.at[n][lines[j], :] for n in range(z_step)], axis=0).astype(BF16)
+            xs[:count, 128 * j:128 * j + 128] = jnp.concatenate(
+                [lay.at[n][lines[j], :] for n in range(len(some_z))], axis=0).astype(BF16)
         phase(f"ffn_in{first_z}")
         for part in range(2):
-            gate = dot(xs[...], eg[part])
-            up = dot(xs[...], eu[part])
-            hid[:, hidden_w * part:hidden_w * (part + 1)] = (silu(gate) * up).astype(BF16)
+            gate = dot(xs[:count], eg[part])
+            up = dot(xs[:count], eu[part])
+            hid[:count, hidden_w * part:hidden_w * (part + 1)] = (silu(gate) * up).astype(BF16)
         phase(f"ffn_out{first_z}")
         for j in range(cols // 2):
             down = ed[:, :, 256 * j:256 * j + 256].reshape(2 * hidden_w, 256)
-            answer = dot(hid[...], down)
-            for n in range(z_step):
+            answer = dot(hid[:count], down)
+            for n in range(len(some_z)):
                 piece = answer[n * b_rows:(n + 1) * b_rows]
                 lay.at[n][lines[2 * j], :] = piece[:, :128]
                 lay.at[n][lines[2 * j + 1], :] = piece[:, 128:]
+        phase(f"back_start{first_z}")
         for n, dz in enumerate(from_z):
             ret_out[pl.ds(dz * block, block)] = lay[n].astype(BF16).reshape(box_shape)
-        phase(f"back_start{first_z}")
-        for dz in from_z:
             each(dz, lambda k: back(dz, k).start())
 
     @pl.when(core == 0)
     def _():
         ret_in[block - 1] = ret_out[block - 1]
 
-    near_z = far_z[::-1]
-    lots = [near_z[:z_step]] + [[dz] for dz in near_z[z_step:]]
+    lots = [list(range(z_step))] + [[dz] for dz in range(z_step, nz)]
     for m, some in enumerate(lots):
         phase(f"back_wait{m}")
         for dz in some:

time: 28.7 us -> 28.1 us (0.979)
  Pallas kernels: 27.9 us -> 27.2 us
    pallas_call x1, Pallas kernels: 27.9 us -> 27.2 us  [per_device(): pl.pallas_call(functools.partial(kernel, dims), out_shape=[jax.ShapeDtype...]
where the time goes in v6:
time: 28.1 us; the launch traced here: 27.9 us
  Pallas kernels  27.2 us (97%)
  other arithmetic  0.66 us (2%)
    pallas_call x1, Pallas kernels, per_device(): pl.pallas_call(functools.partial(kernel, dims), out_shape=[jax.ShapeDtype...  27.2 us
    convert_element_type x1, other arithmetic, per_device(): (residual.astype(F32) + (own.astype(F32) + other.astype(F32))).astype(BF16)  0.66 us

profile of v6, /device:TPU:1, one launch (start us, length us, event | category | flops | bytes accessed | tf_op | source)
XLA Modules:
  0.0 27.9 jit_solution(1704980185589789016)
XLA Ops:
  0.0 27.2 %shard_map.190 = (bf16[16,2048]{1,0:T(8,128)(2,1)S(1)}, bf16[16,2048]{1,0:T(8,128)(2,1)S(1)}, bf16[16,2048]{1,0:T(8,128)(2,1)S(1)}) custom-call(bf16[16,2048]{1,0:T(8,128)(2,1)} %tokens.1, bf16[2048]{0:T(1024)(128)(2,1)} %norm_gain.1, bf16[2048,256]{1,0:T(8,128)(2,1)} %w_query.1, bf16[2048,128]{1,0:T(8,128)(2,1)} %w_key.1, bf16[2048,128]{1,0:T(8,128)(2,1)} %w_value.1, ...), custom_call_target="tpu_custom_call" | custom-call | tf_op jit(solution)/shard_map/pallas_call | solution.py:533
  27.3 0.7 %add_convert_fusion = bf16[16,2048]{1,0:T(8,128)(2,1)} fusion(bf16[16,2048]{1,0:T(8,128)(2,1)S(1)} %get-tuple-element.10, bf16[16,2048]{1,0:T(8,128)(2,1)S(1)} %get-tuple-element.9, bf16[16,2048]{1,0:T(8,128)(2,1)S(1)} %get-tuple-element.8), kind=kLoop, calls=%fused_computation | loop fusion | flops 196608 | bytes 262144 | tf_op jit(solution)/shard_map/convert_element_type | solution.py:542
